TPU v7x, 256 devices: a whole 4x4x8 slice. The times are simulated.
256 devices in a mesh: ep: 64 (over z, y, core), tp: 4 (over x).
Axes of the slice: x: 4, y: 4, z: 8, core: 2. Of those that a mesh axis runs over, the one named last changes fastest.
Arguments:
- conv_value: bfloat16 [24576, 2048], P('ep', 'tp'), may hold values from -36 to 36
- conv_gate: bfloat16 [24576, 2048], P('ep', 'tp'), may hold values from -8 to 8
- conv_taps: bfloat16 [31, 2048], P(None, 'tp'), may hold values from -1 to 1
- conv_gain: float32 [2048], P('tp'), may hold values from 0.1 to 1.9
- conv_proj: bfloat16 [2048, 2048], P('tp'), may hold values from -0.125 to 0.125
- moe_tokens: bfloat16 [24576, 2048], P('ep'), may hold values from -6 to 6
- moe_gain: float32 [2048], replicated, may hold values from 0.1 to 1.9
- routes: int32 [24576, 2], P('ep'), may hold values from 0 to 63, all different within a row; in each aligned block of 384 rows (0 to 383, 384 to 767, ...) at most 18 rows name the same one
- route_weights: float32 [24576, 2], P('ep'), may hold values from 0.3 to 3
- expert_gate: bfloat16 [64, 2048, 1024], P('ep', None, 'tp'), may hold values from -0.125 to 0.125
- expert_up: bfloat16 [64, 2048, 1024], P('ep', None, 'tp'), may hold values from -0.125 to 0.125
- expert_down: bfloat16 [64, 1024, 2048], P('ep', 'tp'), may hold values from -0.1875 to 0.1875
- shared_gate: bfloat16 [2048, 256], replicated, may hold values from -0.125 to 0.125
- shared_up: bfloat16 [2048, 256], replicated, may hold values from -0.125 to 0.125
- shared_down: bfloat16 [256, 2048], P(None, 'tp'), may hold values from -0.375 to 0.375
Outputs:
- conv_result: bfloat16 [24576, 2048], P('ep', 'tp')
- moe_result: bfloat16 [24576, 2048], P('ep', 'tp')
Inputs may be any that keep to these rules, and one draw needn't show every extreme that they name: `routes`: each row names 2 different experts. Among the 384 rows of one index of ep (aligned blocks in order) no expert is named more than 18 times, and in some blocks one expert is named exactly 18 times.
All inputs are finite; a program needn't handle non-finite values.
Results may differ from a plain program's by a relative error of at most 0.01.
Values may be sent and summed in bfloat16 or wider, within the bound.
A program may use at most 64 MiB of HBM per device.

v0:
```python
import jax
import jax.numpy as jnp
from jax import lax
from jax.sharding import PartitionSpec as P

epsilon = 1e-05


def passed_along(value, axis, by):
    devices = lax.axis_size(axis)
    pairs = [(i, i + by) for i in range(devices) if 0 <= i + by < devices]
    return lax.ppermute(value, axis, pairs)


def total_of_pieces(value, axis):
    parts = lax.all_gather(value, axis)
    return parts.sum(axis=0)


def shared_hidden_rows(rows, shared_gate, shared_up):
    return (
        jax.nn.silu(jnp.dot(rows, shared_gate, preferred_element_type=jnp.float32))
        * jnp.dot(rows, shared_up, preferred_element_type=jnp.float32)
    ).astype(jnp.bfloat16)


def local(
    conv_value,
    conv_gate,
    conv_taps,
    conv_gain,
    conv_proj,
    moe_tokens,
    moe_gain,
    routes,
    route_weights,
    expert_gate,
    expert_up,
    expert_down,
    shared_gate,
    shared_up,
    shared_down,
):
    model_width = moe_tokens.shape[1]
    tok_rows = conv_value.shape[0]
    kernel = conv_taps.shape[0]
    gated_rows = (
        conv_value.astype(jnp.float32) * jax.nn.sigmoid(conv_gate.astype(jnp.float32))
    ).astype(jnp.bfloat16)
    previous = passed_along(gated_rows[tok_rows - (kernel - 1) :], "ep", 1)
    padded = jnp.concatenate([previous, gated_rows], axis=0).astype(jnp.float32)
    tap_weights = conv_taps.astype(jnp.float32)
    convolved = jnp.zeros(gated_rows.shape, jnp.float32)
    for offset in range(kernel):
        convolved = convolved + tap_weights[offset][None, :] * padded[offset : offset + tok_rows]
    total_sum, square_sum = (
        total_of_pieces(jnp.sum(convolved, axis=1), "tp"),
        total_of_pieces(jnp.sum(convolved * convolved, axis=1), "tp"),
    )
    average = total_sum / model_width
    variance = square_sum / model_width - average * average
    scaled = (
        (convolved - average[:, None]) * lax.rsqrt(variance + epsilon)[:, None] * conv_gain[None, :]
    )
    activated = jax.nn.silu(scaled).astype(jnp.bfloat16)
    conv_partial = jnp.dot(activated, conv_proj, preferred_element_type=jnp.float32)
    tokens = moe_tokens.astype(jnp.float32)
    token_mean = jnp.mean(tokens, axis=1, keepdims=True)
    centered = tokens - token_mean
    token_var = jnp.mean(centered * centered, axis=1, keepdims=True)
    normalized = (centered * lax.rsqrt(token_var + epsilon) * moe_gain[None, :]).astype(
        jnp.bfloat16
    )
    shared_hidden = shared_hidden_rows(normalized, shared_gate, shared_up)
    shared_part = jnp.dot(shared_hidden, shared_down, preferred_element_type=jnp.float32)
    experts = lax.axis_size("ep")
    top_count = routes.shape[1]
    capacity = 3 * tok_rows * top_count // (2 * experts)
    entries = tok_rows * top_count
    flat_routes = routes.reshape(-1)
    one_hot = (flat_routes[:, None] == jnp.arange(experts, dtype=jnp.int32)[None, :]).astype(
        jnp.int32
    )
    before = jnp.cumsum(one_hot, axis=0) - one_hot
    slot_rank = jnp.sum(before * one_hot, axis=1)
    slot_index = flat_routes * capacity + slot_rank
    source_row = (
        jnp.full((experts * capacity,), -1, jnp.int32)
        .at[slot_index]
        .set(jnp.arange(entries, dtype=jnp.int32))
    )
    filled = source_row >= 0
    token_index = jnp.where(filled, source_row // top_count, 0)
    outgoing = jnp.where(filled[:, None], normalized[token_index], jnp.zeros((), jnp.bfloat16))
    outgoing = outgoing.reshape(experts, capacity, model_width)
    quarter = model_width // lax.axis_size("tp")
    first_column = lax.axis_index("tp") * quarter
    column_block = lax.dynamic_slice_in_dim(outgoing, first_column, quarter, 2)
    arrived = lax.all_to_all(column_block, "ep", split_axis=0, concat_axis=0, tiled=True)
    arrived = lax.all_gather(arrived, "tp", axis=2, tiled=True)
    expert_input = arrived.reshape(experts * capacity, model_width)
    hidden = (
        jax.nn.silu(jnp.dot(expert_input, expert_gate[0], preferred_element_type=jnp.float32))
        * jnp.dot(expert_input, expert_up[0], preferred_element_type=jnp.float32)
    ).astype(jnp.bfloat16)
    expert_partial = jnp.dot(hidden, expert_down[0], preferred_element_type=jnp.float32)
    conv_sum, expert_sum = (
        lax.psum_scatter(
            conv_partial.astype(jnp.bfloat16), "tp", scatter_dimension=1, tiled=True
        ).astype(jnp.float32),
        lax.psum_scatter(
            expert_partial.astype(jnp.bfloat16), "tp", scatter_dimension=1, tiled=True
        ).astype(jnp.float32),
    )
    conv_result = conv_sum.astype(jnp.bfloat16)
    expert_rows = expert_sum.astype(jnp.bfloat16).reshape(experts, capacity, expert_sum.shape[1])
    returned = lax.all_to_all(expert_rows, "ep", split_axis=0, concat_axis=0, tiled=True)
    picked = returned.reshape(experts * capacity, returned.shape[2])[slot_index]
    picked = picked.astype(jnp.float32).reshape(tok_rows, top_count, returned.shape[2])
    moe_result = (shared_part + jnp.sum(route_weights[:, :, None] * picked, axis=1)).astype(
        jnp.bfloat16
    )
    return (conv_result, moe_result)


def solution(mesh):
    placed = (
        P("ep", "tp"),
        P("ep", "tp"),
        P(None, "tp"),
        P("tp"),
        P("tp", None),
        P("ep", None),
        P(),
        P("ep", None),
        P("ep", None),
        P("ep", None, "tp"),
        P("ep", None, "tp"),
        P("ep", "tp", None),
        P(),
        P(),
        P(None, "tp"),
    )
    return jax.shard_map(
        local, mesh=mesh, in_specs=placed, out_specs=(P("ep", "tp"), P("ep", "tp")), check_vma=False
    )
```

profile of v0, /device:TPU:1, one launch (start us, length us, event | category | flops | bytes accessed | tf_op | source)
XLA Modules:
  0.0 311.6 jit_solution(3662823600982574159)
XLA Ops:
  7.2 0.0 copy-start
  7.2 0.0 all-gather.6.cloned.1.call-start
  7.2 1.0 copy.25
  8.2 0.1 eq.29
  8.3 0.1 eq.25
  8.5 0.7 broadcast_multiply_fusion
  9.2 1.8 reduce-window.6
  11.0 0.3 slice_reduce_fusion
  11.3 0.1 copy.24
  11.4 0.2 mul.517
  11.6 0.1 fusion.60
  11.8 3.4 %scatter_custom_fusion = s32[1152]{0:T(1024)S(1)} fusion(s32[768]{0:T(1024)S(1)} %fusion.68, s32[768]{0:T(1024)S(1)} %iota.11, s32[]{:T(128)} %constant.26.clone.1), kind=kCustom, calls=%fused_computation.127 | custom fusion | bytes 4612 | tf_op jit(solution)/shard_map/scatter | solution.py:90
  15.2 0.0 copy-start.1
  15.2 0.0 copy-start.5
  15.2 1.8 convert_reduce_fusion
  17.1 0.0 copy-done.1
  17.1 0.6 fusion.2
  17.6 0.0 copy-done.5
  17.6 1.7 fusion.4
  19.3 12.3 %gather_fusion = bf16[1152,2048]{1,0:T(8,128)(2,1)} fusion(bf16[384,2048]{1,0:T(8,128)(2,1)} %fusion.4, s32[2048]{0:T(1024)S(1)} %pad_clamp_fusion), kind=kCustom, calls=%fused_computation | custom fusion | bytes 9441792 | tf_op jit(solution)/shard_map/gather | solution.py:94
  31.6 7.6 %gather.9 = bf16[64,18,2048]{2,1,0:T(8,128)(2,1)} reshape(bf16[1152,2048]{1,0:T(8,128)(2,1)} %gather_fusion) | data formatting | bytes 9437184 | tf_op jit(solution)/shard_map/gather | solution.py:94
  39.2 0.1 broadcast_in_dim.21
  39.3 1.8 dynamic-slice_select_fusion
  41.2 52.1 %all_to_all.10 = bf16[64,18,512]{2,1,0:T(8,128)(2,1)} all-to-all(bf16[64,18,512]{2,1,0:T(8,128)(2,1)S(1)} %dynamic-slice_select_fusion), channel_id=1, replica_groups=mesh['ep'=64,'tp'=4] {'ep'}, dimensions={0} | all-to-all | bytes 2359296 | tf_op jit(solution)/shard_map/all_to_all | solution.py:99
  93.3 0.0 all-gather.6.cloned.1.call-update
  93.3 0.2 reduce-scatter.5.cloned.1.call-start
  93.5 64.9 %all-gather.6.cloned.1.call-done = bf16[64,18,2048]{2,1,0:T(8,128)(2,1)} async-done(((bf16[64,18,512]{2,1,0:T(8,128)(2,1)}), bf16[64,18,2048]{2,1,0:T(8,128)(2,1)}) %all-gather.6.cloned.1.call-update) | async-done | bytes 4718608 | tf_op jit(solution)/shard_map/all_gather | solution.py:100
  158.5 7.8 %reshape.99 = bf16[1152,2048]{1,0:T(8,128)(2,1)} reshape(bf16[64,18,2048]{2,1,0:T(8,128)(2,1)} %all-gather.6.cloned.1.call-done) | data formatting | bytes 9437184 | tf_op jit(solution)/shard_map/reshape | solution.py:101
  166.2 5.1 %fusion.16 = f32[1152,256]{1,0:T(8,128)} fusion(bf16[1152,2048]{1,0:T(8,128)(2,1)} %reshape.99, bf16[1,2048,256]{2,1,0:T(8,128)(2,1)} %param.24), kind=kOutput, calls=%fused_computation.27 | convolution fusion | flops 1207959552 | bytes 6946816 | tf_op jit(solution)/shard_map/dot_general | solution.py:103
  171.3 10.3 %convolution_convert_fusion = bf16[1152,2048]{1,0:T(8,128)(2,1)} fusion(bf16[1152,2048]{1,0:T(8,128)(2,1)} %reshape.99, f32[1152,256]{1,0:T(8,128)} %fusion.16, bf16[1,256,2048]{2,1,0:T(8,128)(2,1)} %param.26, bf16[1,2048,256]{2,1,0:T(8,128)(2,1)} %param.25), kind=kOutput, calls=%fused_computation.3 | convolution fusion | flops 2420047872 | bytes 12713984 | tf_op jit(solution)/shard_map/dot_general | solution.py:106
  181.6 0.0 copy-start.2
  181.6 0.0 copy-start.3
  181.6 0.0 copy-start.4
  181.6 0.0 reduce-scatter.5.cloned.1.call-update
  181.6 0.0 reduce-scatter.3.cloned.1.call-start
  181.7 0.9 copy-done.2
  182.6 0.1 copy-done.3
  182.7 0.2 multiply_convert_fusion.1
  182.9 3.8 %collective-permute-start = (bf16[30,512]{1,0:T(8,128)(2,1)S(1)}, bf16[30,512]{1,0:T(8,128)(2,1)S(1)}, u32[]{:S(2)}, u32[]{:S(2)}) collective-permute-start(bf16[30,512]{1,0:T(8,128)(2,1)S(1)} %slice.265), channel_id=1, source_target_pairs={{0,4},{4,8},{8,12},{12,16},{16,20},{20,24},{24,28},{28,32},{32,36}... | collective-permute-start | bytes 92168 | tf_op jit(solution)/shard_map/ppermute | solution.py:12
  186.8 0.0 copy-done.4
  186.9 0.9 collective-permute-done
  187.8 0.1 maximum_convert_fusion
  187.9 0.0 copy-start.8
  187.9 3.8 %fusion.72 = (f32[384]{0:T(512)S(1)}, f32[384]{0:T(512)S(1)}, f32[384,512]{1,0:T(8,128)S(1)}) fusion(f32[414,512]{1,0:T(8,128)S(1)} %maximum_convert_fusion, f32[512]{0:T(512)S(1)} %bitcast.100, f32[512]{0:T(512)S(1)} %bitcast.99, f32[512]{0:T(512)S(1)} %bitcast.98, f32[512]{0:T(512)S(1)} %bitcast.97, f32[512]{0:T(512)S(1)} %bitcast.96, ...), kind=kLoop, calls=%fused_computation.138 | loop fusion | flops 12582144 | bytes 25232384 | tf_op jit(solution)/shard_map/reduce_sum | solution.py:57
  191.8 9.1 %all-gather.2 = f32[4,1,384]{2,1,0:T(1,128)S(1)} all-gather(f32[1,1,384]{2,1,0:T(1,128)S(1)} %reshape.130), channel_id=2, replica_groups=mesh['ep'=64,'tp'=4] {'tp'}, dimensions={0}, use_global_device_ids=true | all-gather | bytes 7680 | tf_op jit(solution)/shard_map/all_gather | solution.py:16
  200.9 9.6 %all-gather.3 = f32[4,1,384]{2,1,0:T(1,128)S(1)} all-gather(f32[1,1,384]{2,1,0:T(1,128)S(1)} %reshape.132), channel_id=3, replica_groups=mesh['ep'=64,'tp'=4] {'tp'}, dimensions={0}, use_global_device_ids=true | all-gather | bytes 7680 | tf_op jit(solution)/shard_map/all_gather | solution.py:16
  210.5 0.0 copy-done
  210.5 0.0 copy-done.8
  210.5 2.3 convolution_convert_fusion.1
  212.8 0.0 reduce-scatter.3.cloned.1.call-update
  212.9 23.5 %reduce-scatter.5.cloned.1.call-done = bf16[1152,512]{1,0:T(8,128)(2,1)} async-done(((bf16[1152,2048]{1,0:T(8,128)(2,1)}), bf16[1152,512]{1,0:T(8,128)(2,1)}) %reduce-scatter.5.cloned.1.call-update) | async-done | bytes 1179664 | tf_op jit(solution)/shard_map/reduce_scatter | solution.py:111
  236.4 3.0 reshape.100
  239.4 11.1 %all-to-all-start.1 = ((bf16[64,18,512]{2,1,0:T(8,128)(2,1)}), bf16[64,18,512]{2,1,0:T(8,128)(2,1)}, u32[]{:S(2)}, u32[]{:S(2)}) async-start(bf16[64,18,512]{2,1,0:T(8,128)(2,1)} %reshape.100), calls=%async_computation.3 | async-start | bytes 3145728 | tf_op jit(solution)/shard_map/all_to_all | solution.py:117
  250.5 0.0 copy-done.6
  250.5 0.1 copy.23
  250.7 3.1 fusion.76
  253.7 35.8 %all-to-all-done.1 = bf16[64,18,512]{2,1,0:T(8,128)(2,1)} async-done(((bf16[64,18,512]{2,1,0:T(8,128)(2,1)}), bf16[64,18,512]{2,1,0:T(8,128)(2,1)}, u32[]{:S(2)}, u32[]{:S(2)}) %all-to-all-start.1) | async-done | bytes 1179680 | tf_op jit(solution)/shard_map/all_to_all | solution.py:117
  289.5 2.3 reshape.101
  291.8 3.3 %gather_fusion.1 = bf16[768,512]{1,0:T(8,128)(2,1)} fusion(bf16[1152,512]{1,0:T(8,128)(2,1)S(1)} %reshape.101, s32[1024]{0:T(1024)S(1)} %pad_clamp_fusion.1), kind=kCustom, calls=%fused_computation.1 | custom fusion | bytes 1575936 | tf_op jit(solution)/shard_map/gather | solution.py:118
  295.1 3.0 reshape.102
  298.1 0.0 copy-start.7
  298.1 3.6 %multiply_reduce_fusion = f32[384,512]{1,0:T(8,128)S(1)} fusion(f32[384,2,512]{2,1,0:T(2,128)} %reshape.102, f32[384,2]{1,0:T(8,128)S(1)} %copy.23), kind=kLoop, calls=%fused_computation.15 | loop fusion | flops 589824 | bytes 2362368 | tf_op jit(solution)/shard_map/reduce_sum | solution.py:120
  301.7 0.0 copy-done.7
  301.7 3.4 %fusion.6 = bf16[384,512]{1,0:T(8,128)(2,1)} fusion(f32[384,512]{1,0:T(8,128)S(1)} %multiply_reduce_fusion, bf16[256,512]{1,0:T(8,128)(2,1)S(1)} %copy-done.7, bf16[384,2048]{1,0:T(8,128)(2,1)} %fusion.4, bf16[2048,256]{1,0:T(8,128)(2,1)} %param.28, f32[384,256]{1,0:T(8,128)} %fusion.76), kind=kOutput, calls=%fused_computation.17 | convolution fusion | flops 504299520 | bytes 4456448 | tf_op jit(solution)/shard_map/dot_general | solution.py:75
  (20 shorter events, 0.2 us)
Async XLA Ops:
  7.2 203.3 %copy-start = (bf16[512,2048]{1,0:T(8,128)(2,1)S(1)}, bf16[512,2048]{1,0:T(8,128)(2,1)}, u32[]{:S(2)}) copy-start(bf16[512,2048]{1,0:T(8,128)(2,1)} %param.19) | copy-start | bytes 6291460
  7.2 151.3 %all-gather.6.cloned.1.call-start = ((), (), s32[]{:S(2)}) async-start(), calls=%async_computation.5 | async-start | bytes 7864320 | tf_op jit(solution)/shard_map/all_gather | solution.py:100
  15.2 1.9 copy-start.1
  15.2 2.4 copy-start.5
  93.3 143.1 %reduce-scatter.5.cloned.1.call-start = ((), (), s32[]{:S(2)}) async-start(), calls=%async_computation.6 | async-start | bytes 5898240 | tf_op jit(solution)/shard_map/reduce_scatter | solution.py:111
  181.6 1.0 copy-start.2
  181.6 1.1 copy-start.3
  181.6 5.2 %copy-start.4 = (bf16[31,512]{1,0:T(8,128)(2,1)S(1)}, bf16[31,512]{1,0:T(8,128)(2,1)}, u32[]{:S(2)}) copy-start(bf16[31,512]{1,0:T(8,128)(2,1)} %param.17) | copy-start | bytes 95236
  181.6 123.5 %reduce-scatter.3.cloned.1.call-start = ((), (), s32[]{:S(2)}) async-start(), calls=%async_computation.4 | async-start | bytes 1966080 | tf_op jit(solution)/shard_map/reduce_scatter | solution.py:108
  182.9 4.9 %collective-permute-start = (bf16[30,512]{1,0:T(8,128)(2,1)S(1)}, bf16[30,512]{1,0:T(8,128)(2,1)S(1)}, u32[]{:S(2)}, u32[]{:S(2)}) collective-permute-start(bf16[30,512]{1,0:T(8,128)(2,1)S(1)} %slice.265), channel_id=1, source_target_pairs={{0,4},{4,8},{8,12},{12,16},{16,20},{20,24},{24,28},{28,32},{32,36}... | collective-permute-start | bytes 92168 | tf_op jit(solution)/shard_map/ppermute | solution.py:12
  187.9 22.6 %copy-start.8 = (f32[512]{0:T(512)S(1)}, f32[512]{0:T(512)}, u32[]{:S(2)}) copy-start(f32[512]{0:T(512)} %param.18) | copy-start | bytes 6148
  239.4 11.1 %copy-start.6 = (f32[384,2]{0,1:T(2,128)S(1)}, f32[384,2]{0,1:T(2,128)}, u32[]{:S(2)}) copy-start(f32[384,2]{0,1:T(2,128)} %param.23) | copy-start | bytes 9220
  239.4 50.1 %all-to-all-start.1 = ((bf16[64,18,512]{2,1,0:T(8,128)(2,1)}), bf16[64,18,512]{2,1,0:T(8,128)(2,1)}, u32[]{:S(2)}, u32[]{:S(2)}) async-start(bf16[64,18,512]{2,1,0:T(8,128)(2,1)} %reshape.100), calls=%async_computation.3 | async-start | bytes 3145728 | tf_op jit(solution)/shard_map/all_to_all | solution.py:117
  298.1 3.6 %copy-start.7 = (bf16[256,512]{1,0:T(8,128)(2,1)S(1)}, bf16[256,512]{1,0:T(8,128)(2,1)}, u32[]{:S(2)}) copy-start(bf16[256,512]{1,0:T(8,128)(2,1)} %param.29) | copy-start | bytes 786436
Sparse Core Ops, SparseCore 0:
  93.4 65.0 all-gather.5
  181.7 54.6 reduce-scatter.4
  239.5 27.0 reduce-scatter.2
where the time goes:
time: 313 us; the launch traced here: 312 us
  waiting for transfers between devices  125 us (40%)
  blocking collectives  70.7 us (23%)
  local copies, waits for them, and re-layouts  45.9 us (15%)
  matrix products  24.2 us (8%)
  other arithmetic  16.4 us (5%)
  starting transfers between devices  15.2 us (5%)
  between operations  14 us (4%)
    all_gather x1, waiting for transfers between devices, local(): arrived = lax.all_gather(arrived, 'tp', axis=2, tiled=True)  64.9 us
    all_to_all x1, blocking collectives, local(): lax.all_to_all(column_block, 'ep', split_axis=0, concat_axis=0, tiled=True)  52.1 us
    all_to_all x1, waiting for transfers between devices, local(): lax.all_to_all(expert_rows, 'ep', split_axis=0, concat_axis=0, tiled=True)  35.8 us
    reduce_scatter x1, waiting for transfers between devices, local(): lax.psum_scatter(expert_partial.astype(jnp.bfloat16), 'tp', scatter_dimen...  23.5 us
    gather x2, local copies, waits for them, and re-layouts, local(): normalized[token_index]  19.9 us
    all_gather x2, blocking collectives, total_of_pieces(): parts = lax.all_gather(value, axis)  18.6 us
    all_to_all x1, starting transfers between devices, local(): lax.all_to_all(expert_rows, 'ep', split_axis=0, concat_axis=0, tiled=True)  11.1 us
    dot_general x1, matrix products, local(): jnp.dot(hidden, expert_down[0], preferred_element_type=jnp.float32)  10.3 us
  transfers between devices with their start and end apart: 5, of which 4 were waited for; matrix products, arithmetic and copies ran while one was open for 9% of the time, Pallas kernels for 0%

commit v1 on v0

v1 whole, which is shorter than its diff:
```python
import functools

import jax
import jax.numpy as jnp
from jax import lax
from jax.experimental import pallas as pl
from jax.experimental.pallas import tpu as pltpu
from jax.sharding import PartitionSpec as P

MESH = pl.DeviceIdType.MESH
F32 = jnp.float32
BF16 = jnp.bfloat16
epsilon = 1e-05

ORDER = (0, 1, 7, 2, 6, 3, 5, 4)
PLANE = 8
MAIN = 16
REST = 2
ROWS = PLANE * (MAIN + REST)
BODY = PLANE * MAIN
NEAR = 3
BATCHES = ((0, 3), (7, 1), (5, 2), (3, 2))


def silu(v):
    return v / (1.0 + jnp.exp(-v))


def dot(a, b):
    return jnp.dot(a, b, preferred_element_type=F32)


def iota(shape, dim):
    return lax.broadcasted_iota(jnp.int32, shape, dim)


def kernel(
    cv_hbm,
    cg_hbm,
    taps_ref,
    cgain_ref,
    cproj_hbm,
    tok_hbm,
    mgain_ref,
    routes_ref,
    weights_ref,
    eg_hbm,
    eu_hbm,
    ed_hbm,
    sg_hbm,
    su_hbm,
    sd_hbm,
    conv_out,
    moe_out,
    cv,
    cg,
    cproj,
    tok,
    wg,
    wu,
    sg,
    su,
    sd,
    norm,
    send_near,
    send_near_rest,
    send_far,
    send_far_rest,
    xin,
    in_near_rest,
    in_far_rest,
    hid,
    down,
    down_pass,
    back_send,
    back_send_rest,
    back,
    back_rest,
    total,
    padded,
    taps,
    conv,
    ssum,
    ssq,
    tail,
    halo,
    stat_send,
    stat,
    act,
    cfar,
    cright,
    cleft,
    cown,
    half_a,
    half_b,
    from_left,
    from_right,
    load_sem,
    go_send,
    go_recv,
    go_rest_send,
    go_rest_recv,
    back_ssem,
    back_rsem,
    back_rest_ssem,
    back_rest_rsem,
    ag_send,
    ag_recv,
    down_send,
    down_recv,
    halo_send,
    halo_recv,
    stat_ssem,
    stat_rsem,
    rs_send,
    rs_recv,
):
    ep, tp = lax.axis_index("ep"), lax.axis_index("tp")
    n_ep, n_tp = lax.axis_size("ep"), lax.axis_size("tp")
    planes = n_ep // PLANE
    z, mine = ep // PLANE, lax.rem(ep, PLANE)
    right, left, across = (lax.rem(tp + i, n_tp) for i in (1, 3, 2))
    tokens, width = tok.shape
    quarter = width // n_tp
    ff = wg.shape[1]

    def remote(src, dst, ssem, rsem, to_ep, to_tp):
        return pltpu.make_async_remote_copy(
            src_ref=src,
            dst_ref=dst,
            send_sem=ssem,
            recv_sem=rsem,
            device_id=(to_ep, to_tp),
            device_id_type=MESH,
        )

    def arrived(ref, sem):
        remote(ref, ref, sem, sem, ep, right).wait_recv()

    def left_here(ref, sem):
        remote(ref, ref, sem, sem, ep, right).wait_send()

    barrier = pltpu.get_barrier_semaphore()

    @pl.loop(1, n_ep)
    def _(o):
        pl.semaphore_signal(
            barrier, inc=1, device_id=(lax.rem(ep + o, n_ep), tp), device_id_type=MESH
        )

    for peer in (right, left, across):
        pl.semaphore_signal(barrier, inc=1, device_id=(ep, peer), device_id_type=MESH)

    def at_quarter(q):
        return pl.ds(pl.multiple_of(q * quarter, quarter), quarter)

    def at_ff(q):
        return pl.ds(pl.multiple_of(q * ff, ff), ff)

    loads = {}
    for number, (name, src, dst) in enumerate(
        (
            ("tok", tok_hbm, tok),
            ("cv", cv_hbm, cv),
            ("cg", cg_hbm, cg),
            ("sg", sg_hbm, sg),
            ("su", su_hbm, su),
            ("sd", sd_hbm, sd),
            ("cproj", cproj_hbm, cproj),
            ("wg", eg_hbm.at[0], wg),
            ("wu", eu_hbm.at[0], wu),
            ("down", ed_hbm.at[0, :, at_quarter(tp)], down.at[at_ff(tp)]),
        )
    ):
        loads[name] = pltpu.make_async_copy(src, dst, load_sem.at[number])
        loads[name].start()

    loads["cv"].wait()
    loads["cg"].wait()
    blocks = quarter // 128
    extra = halo.shape[0]
    for b in range(blocks):
        lanes = slice(b * 128, (b + 1) * 128)
        gated = (cv[:, lanes].astype(F32) * jax.nn.sigmoid(cg[:, lanes].astype(F32))).astype(BF16)
        padded[b, extra:, :] = gated.astype(F32)
        tail[:, lanes] = gated[tokens - extra :]
        taps[b, 0:31] = taps_ref[:, lanes].astype(F32)

    loads["tok"].wait()
    for r in range(0, tokens, 64):
        rows = tok[r : r + 64, :].astype(F32)
        mean = jnp.sum(rows, axis=1, keepdims=True) * (1.0 / width)
        centered = rows - mean
        var = jnp.sum(centered * centered, axis=1, keepdims=True) * (1.0 / width)
        norm[r : r + 64, :] = (centered * lax.rsqrt(var + epsilon) * mgain_ref[...]).astype(BF16)

    pl.semaphore_wait(barrier, n_ep - 1 + n_tp - 1)

    next_ep = lax.rem(ep + 1, n_ep)
    remote(tail, halo, halo_send, halo_recv, next_ep, tp).start()

    half = ff // 2

    def down_rows(owner, first, count):
        return down.at[pl.ds(pl.multiple_of(owner * ff + first, half), count)]

    ed = ed_hbm.at[0]
    remote(ed.at[:, at_quarter(right)], down_rows(tp, 0, ff), down_send.at[0], down_recv.at[0], ep, right).start()
    remote(ed.at[:, at_quarter(left)], down_rows(tp, 0, ff), down_send.at[1], down_recv.at[1], ep, left).start()
    remote(ed.at[0:half, at_quarter(across)], down_pass.at[0], down_send.at[2], down_recv.at[2], ep, right).start()
    remote(ed.at[half:ff, at_quarter(across)], down_pass.at[1], down_send.at[3], down_recv.at[3], ep, left).start()

    routes = routes_ref[...]
    first, second = routes[0:1, :], routes[1:2, :]
    names = iota((n_ep, tokens), 0)
    is_first = (names == first).astype(F32)
    is_second = (names == second).astype(F32)
    earlier = (iota((tokens, tokens), 0) < iota((tokens, tokens), 1)).astype(F32).astype(BF16)
    before = dot((is_first + is_second).astype(BF16), earlier)

    def slot_of(route, chosen):
        rank = jnp.sum(before * chosen, axis=0, keepdims=True).astype(jnp.int32)
        away = ((route >> 3) - z + planes) & (planes - 1)
        place = route & (PLANE - 1)
        group = jnp.where(away == 0, 0, jnp.where(away <= 4, 2 * away - 1, 2 * (planes - away)))
        inside = jnp.where(rank < MAIN, place * MAIN + rank, BODY + place * REST + rank - MAIN)
        return group * ROWS + inside

    slot_first, slot_second = slot_of(first, is_first), slot_of(second, is_second)

    way = iota((64, 64), 0)
    here = iota((64, 64), 1)
    same = (way >> 3 == (here >> 1 & 7)) & ((way >> 1 & 3) == here >> 4) & ((way & 1) == (here & 1))
    to_way = same.astype(F32).astype(BF16)
    way = iota((64, 64), 1)
    here = iota((64, 64), 0)
    same = (way >> 3 == (here >> 1 & 7)) & ((way >> 1 & 3) == here >> 4) & ((way & 1) == (here & 1))
    to_here = same.astype(F32).astype(BF16)

    def pack_rest(rest):
        n = rest.shape[1] // 512
        stacked = jnp.concatenate(
            [
                jnp.concatenate(
                    [rest[:, q * 512 + g * 128 : q * 512 + (g + 1) * 128] for q in range(n)], axis=1
                )
                for g in range(4)
            ],
            axis=0,
        )
        return dot(to_way, stacked.astype(BF16)).reshape(8, 8, n * 128)

    def unpack_rest(packed):
        n = packed.shape[2] // 128
        stacked = dot(to_here, packed.astype(F32).reshape(64, n * 128).astype(BF16))
        return jnp.concatenate(
            [
                stacked[g * 16 : (g + 1) * 16, q * 128 : (q + 1) * 128]
                for q in range(n)
                for g in range(4)
            ],
            axis=1,
        ).astype(BF16)

    def row_of(group, place, count=MAIN):
        return pl.ds(pl.multiple_of(group * ROWS + place * MAIN, MAIN), count)

    def place_rows(place):
        return pl.ds(pl.multiple_of(place * MAIN, MAIN), MAIN)

    def exchange(group, sign, main, main_at, rest, rest_at, ssem, rsem, rest_ssem, rest_rsem):
        plane = lax.rem(z + sign * ORDER[group] + planes, planes)

        @pl.loop(1 if group == 0 else 0, PLANE)
        def _(o):
            place = lax.rem(mine + o, PLANE)
            to = plane * PLANE + place
            remote(main.at[place_rows(place)], main_at, ssem.at[group], rsem.at[group], to, tp).start()
            remote(rest.at[place], rest_at, rest_ssem.at[group], rest_rsem.at[group], to, tp).start()

    def sent_or_come(group, wait, main, rest, sem, rest_sem):
        count = PLANE - 1 if group == 0 else PLANE
        wait(main.at[0 : count * MAIN], sem.at[group])
        wait(rest.at[0:count], rest_sem.at[group])

    def far_lanes():
        return at_quarter(tp)

    for group in (0, 1, 2, 7, 5, 6, 3, 4):
        row = iota((ROWS, tokens), 0) + group * ROWS
        pick = ((row == slot_first) | (row == slot_second)).astype(F32).astype(BF16)
        if group < NEAR:
            rows = dot(pick, norm[...])
            send_near[group] = rows[0:BODY].astype(BF16)
            send_near_rest[group] = pack_rest(rows[BODY:]).astype(BF16)
            main, rest = send_near.at[group], send_near_rest.at[group]
            main_at, rest_at = xin.at[row_of(group, mine)], in_near_rest.at[group, mine]
        else:
            rows = dot(pick, norm[:, far_lanes()])
            send_far[group - NEAR] = rows[0:BODY].astype(BF16)
            send_far_rest[group - NEAR] = pack_rest(rows[BODY:]).astype(BF16)
            main, rest = send_far.at[group - NEAR], send_far_rest.at[group - NEAR]
            main_at = xin.at[row_of(group, mine), far_lanes()]
            rest_at = in_far_rest.at[group - NEAR, mine]
        exchange(group, 1, main, main_at, rest, rest_at, go_send, go_recv, go_rest_send, go_rest_recv)
        if group == 0:
            xin[row_of(0, mine), :] = send_near[0, place_rows(mine), :]
            in_near_rest[0, mine] = send_near_rest[0, mine]

    arrived(halo, halo_recv)
    for b in range(blocks):
        before_rows = halo[:, b * 128 : (b + 1) * 128].astype(F32)
        padded[b, 0:extra, :] = jnp.where(ep == 0, jnp.zeros_like(before_rows), before_rows)
    ssum[...] = jnp.zeros_like(ssum)
    ssq[...] = jnp.zeros_like(ssq)

    @pl.loop(0, blocks)
    def _(b):
        for r in range(0, tokens, 64):
            acc = jnp.zeros((64, 128), F32)
            for offset in range(31):
                start = r + offset + extra - 30
                acc = acc + taps[b, offset : offset + 1, :] * padded[b, start : start + 64, :]
            conv[b, r : r + 64, :] = acc
            ssum[r : r + 64, :] += acc
            ssq[r : r + 64, :] += acc * acc

    eighth = iota((8, tokens), 0)
    sums = jnp.sum(ssum[...].T, axis=0, keepdims=True)
    squares = jnp.sum(ssq[...].T, axis=0, keepdims=True)
    own_stat = jnp.where(eighth == 0, sums, jnp.where(eighth == 1, squares, 0.0))
    stat_send[...] = own_stat
    stat[tp] = own_stat
    for i, peer in enumerate((right, left, across)):
        remote(stat_send, stat.at[tp], stat_ssem.at[i], stat_rsem.at[i], ep, peer).start()

    loads["sg"].wait()
    loads["su"].wait()
    loads["sd"].wait()
    shared = (silu(dot(norm[...], sg[...])) * dot(norm[...], su[...])).astype(BF16)
    total[...] = dot(shared, sd[...])

    for i, peer in enumerate((left, right, across)):
        arrived(stat.at[peer], stat_rsem.at[i])
    sums = stat[0] + stat[1] + stat[2] + stat[3]
    average = sums[0:1] * (1.0 / width)
    variance = sums[1:2] * (1.0 / width) - average * average
    scale = lax.rsqrt(variance + epsilon)
    tall = iota((128, tokens), 0)
    turned = jnp.where(tall == 0, average, jnp.where(tall == 1, scale, 0.0)).T
    average, scale = turned[:, 0:1], turned[:, 1:2]
    for b in range(blocks):
        lanes = slice(b * 128, (b + 1) * 128)
        act[:, lanes] = silu((conv[b] - average) * scale * cgain_ref[:, lanes]).astype(BF16)

    loads["cproj"].wait()
    upper = tokens // 2
    top, bottom = slice(0, upper), slice(upper, tokens)

    def product(q):
        return dot(act[...], cproj[:, at_quarter(q)])

    cfar[...] = product(across).astype(BF16)
    remote(cfar.at[top], half_a, rs_send.at[0], rs_recv.at[0], ep, right).start()
    remote(cfar.at[bottom], half_b, rs_send.at[1], rs_recv.at[1], ep, left).start()
    cright[...] = product(right).astype(BF16)
    remote(cright.at[bottom], from_left.at[bottom], rs_send.at[2], rs_recv.at[2], ep, right).start()
    cleft[...] = product(left).astype(BF16)
    remote(cleft.at[top], from_right.at[top], rs_send.at[3], rs_recv.at[3], ep, left).start()
    cown[...] = product(tp)

    arrived(down_pass.at[0], down_recv.at[2])
    remote(down_pass.at[0], down_rows(left, 0, half), down_send.at[4], down_recv.at[4], ep, right).start()
    arrived(down_pass.at[1], down_recv.at[3])
    remote(down_pass.at[1], down_rows(right, half, half), down_send.at[5], down_recv.at[5], ep, left).start()

    arrived(half_a, rs_recv.at[0])
    cright[top] = (cright[top].astype(F32) + half_a[...].astype(F32)).astype(BF16)
    remote(cright.at[top], from_left.at[top], rs_send.at[4], rs_recv.at[4], ep, right).start()
    arrived(half_b, rs_recv.at[1])
    cleft[bottom] = (cleft[bottom].astype(F32) + half_b[...].astype(F32)).astype(BF16)
    remote(cleft.at[bottom], from_right.at[bottom], rs_send.at[5], rs_recv.at[5], ep, left).start()

    def parts_of(count):
        cut = (count // 2 + 15) // 16 * 16
        return (0, cut), (cut, count - cut)

    def region(ref, lanes, first, rows, q):
        return ref.at[first : first + rows, lanes(q)]

    def gather_start(i, ref, lanes, first, count):
        own = region(ref, lanes, first, count, tp)
        remote(own, own, ag_send.at[i, 0], ag_recv.at[i, 0], ep, right).start()
        remote(own, own, ag_send.at[i, 1], ag_recv.at[i, 1], ep, left).start()

    def gather_pass(i, ref, lanes, first, count):
        (a, na), (b, nb) = parts_of(count)
        arrived(region(ref, lanes, first, count, left), ag_recv.at[i, 0])
        half = region(ref, lanes, first + a, na, left)
        remote(half, half, ag_send.at[i, 2], ag_recv.at[i, 2], ep, right).start()
        arrived(region(ref, lanes, first, count, right), ag_recv.at[i, 1])
        half = region(ref, lanes, first + b, nb, right)
        remote(half, half, ag_send.at[i, 3], ag_recv.at[i, 3], ep, left).start()

    def gather_end(i, ref, lanes, first, count):
        (a, na), (b, nb) = parts_of(count)
        arrived(region(ref, lanes, first + a, na, across), ag_recv.at[i, 2])
        arrived(region(ref, lanes, first + b, nb, across), ag_recv.at[i, 3])

    def gather_sent(i, ref, lanes, first, count):
        (a, na), (b, nb) = parts_of(count)
        left_here(region(ref, lanes, first, count, tp), ag_send.at[i, 0])
        left_here(region(ref, lanes, first, count, tp), ag_send.at[i, 1])
        left_here(region(ref, lanes, first + a, na, left), ag_send.at[i, 2])
        left_here(region(ref, lanes, first + b, nb, right), ag_send.at[i, 3])

    def of_batch(batch):
        first, count = BATCHES[batch]
        return first * ROWS, count * ROWS

    def rows_gather(step, batch):
        step(batch, xin, at_quarter, *of_batch(batch))

    def hidden_gather(step, batch):
        step(len(BATCHES) + batch, hid, at_ff, *of_batch(batch))

    def come(batch):
        first, count = BATCHES[batch]
        for group in range(first, first + count):
            start = group * ROWS
            if group < NEAR:
                main, rest = xin.at[start : start + BODY], in_near_rest.at[group]
            else:
                main, rest = xin.at[start : start + BODY, far_lanes()], in_far_rest.at[group - NEAR]
            sent_or_come(group, arrived, main, rest, go_recv, go_rest_recv)
            if group < NEAR:
                xin[start + BODY : start + ROWS, :] = unpack_rest(rest[...])
            else:
                xin[start + BODY : start + ROWS, far_lanes()] = unpack_rest(rest[...])

    def hidden(batch):
        first, count = of_batch(batch)
        rows = xin[first : first + count, :]
        value = silu(dot(rows, wg[...])) * dot(rows, wu[...])
        hid[first : first + count, at_ff(tp)] = value.astype(BF16)

    def send_back(batch):
        first, count = BATCHES[batch]
        start = first * ROWS
        rows = dot(hid[start : start + count * ROWS, :], down[...])
        for group in range(first, first + count):
            own = rows[(group - first) * ROWS : (group - first + 1) * ROWS]
            back_send[group] = own[0:BODY].astype(BF16)
            back_send_rest[group] = pack_rest(own[BODY:]).astype(BF16)
            exchange(
                group,
                -1,
                back_send.at[group],
                back.at[row_of(group, mine)],
                back_send_rest.at[group],
                back_rest.at[group, mine],
                back_ssem,
                back_rsem,
                back_rest_ssem,
                back_rest_rsem,
            )
            if group == 0:
                back[row_of(0, mine), :] = back_send[0, place_rows(mine), :]
                back_rest[0, mine] = back_send_rest[0, mine]

    wide = jnp.where(tall == 0, slot_first.astype(F32), jnp.where(tall == 1, slot_second.astype(F32), 0.0))
    given = weights_ref[...]
    wide = jnp.where(tall == 2, given[0:1, :], jnp.where(tall == 3, given[1:2, :], wide))
    turned = wide.T
    slot_one, slot_two = turned[:, 0:1].astype(jnp.int32), turned[:, 1:2].astype(jnp.int32)
    weight_one, weight_two = turned[:, 2:3], turned[:, 3:4]

    def combine(batch):
        first, count = BATCHES[batch]
        for group in range(first, first + count):
            start = group * ROWS
            sent_or_come(
                group, arrived, back.at[start : start + BODY], back_rest.at[group], back_rsem, back_rest_rsem
            )
            back[start + BODY : start + ROWS, :] = unpack_rest(back_rest[group])
        start = first * ROWS
        lane = iota((tokens, count * ROWS), 1) + start
        mix = jnp.where(lane == slot_one, weight_one, 0.0) + jnp.where(lane == slot_two, weight_two, 0.0)
        high = mix.astype(BF16)
        low = (mix - high.astype(F32)).astype(BF16)
        rows = back[start : start + count * ROWS, :]
        total[...] += dot(high, rows) + dot(low, rows)

    come(0)
    loads["wg"].wait()
    loads["wu"].wait()
    hidden(0)
    hidden_gather(gather_start, 0)
    come(1)
    rows_gather(gather_start, 1)
    hidden_gather(gather_pass, 0)
    come(2)
    rows_gather(gather_start, 2)
    rows_gather(gather_pass, 1)
    come(3)
    rows_gather(gather_start, 3)

    loads["down"].wait()
    arrived(down_rows(left, 0, ff), down_recv.at[0])
    arrived(down_rows(right, 0, ff), down_recv.at[1])
    arrived(down_rows(across, 0, half), down_recv.at[4])
    arrived(down_rows(across, half, half), down_recv.at[5])
    hidden_gather(gather_end, 0)
    send_back(0)

    rows_gather(gather_end, 1)
    hidden(1)
    hidden_gather(gather_start, 1)
    rows_gather(gather_pass, 2)
    rows_gather(gather_pass, 3)
    rows_gather(gather_end, 2)
    hidden(2)
    hidden_gather(gather_start, 2)
    hidden_gather(gather_pass, 1)
    hidden_gather(gather_end, 1)
    send_back(1)
    rows_gather(gather_end, 3)
    hidden(3)
    hidden_gather(gather_start, 3)
    hidden_gather(gather_pass, 2)
    hidden_gather(gather_end, 2)
    send_back(2)
    hidden_gather(gather_pass, 3)

    arrived(from_left.at[bottom], rs_recv.at[2])
    arrived(from_right.at[top], rs_recv.at[3])
    arrived(from_left.at[top], rs_recv.at[4])
    arrived(from_right.at[bottom], rs_recv.at[5])
    conv_out[...] = (cown[...] + from_left[...].astype(F32) + from_right[...].astype(F32)).astype(BF16)

    combine(0)
    hidden_gather(gather_end, 3)
    send_back(3)
    combine(1)
    combine(2)
    combine(3)
    moe_out[...] = total[...].astype(BF16)

    left_here(tail, halo_send)
    left_here(ed.at[:, at_quarter(right)], down_send.at[0])
    left_here(ed.at[:, at_quarter(left)], down_send.at[1])
    left_here(ed.at[0:half, at_quarter(across)], down_send.at[2])
    left_here(ed.at[half:ff, at_quarter(across)], down_send.at[3])
    left_here(down_pass.at[0], down_send.at[4])
    left_here(down_pass.at[1], down_send.at[5])
    for i in range(3):
        left_here(stat_send, stat_ssem.at[i])
    for i, part in enumerate((cfar.at[top], cfar.at[bottom], cright.at[bottom], cleft.at[top], cright.at[top], cleft.at[bottom])):
        left_here(part, rs_send.at[i])
    for group in range(len(ORDER)):
        if group < NEAR:
            main, rest = send_near.at[group], send_near_rest.at[group]
        else:
            main, rest = send_far.at[group - NEAR], send_far_rest.at[group - NEAR]
        sent_or_come(group, left_here, main, rest, go_send, go_rest_send)
        sent_or_come(group, left_here, back_send.at[group], back_send_rest.at[group], back_ssem, back_rest_ssem)
    for batch in range(len(BATCHES)):
        if batch > 0:
            rows_gather(gather_sent, batch)
        hidden_gather(gather_sent, batch)


def local(
    conv_value,
    conv_gate,
    conv_taps,
    conv_gain,
    conv_proj,
    moe_tokens,
    moe_gain,
    routes,
    route_weights,
    expert_gate,
    expert_up,
    expert_down,
    shared_gate,
    shared_up,
    shared_down,
):
    tokens, width = moe_tokens.shape
    quarter = conv_value.shape[1]
    ff = expert_gate.shape[2]
    full_ff = ff * lax.axis_size("tp")
    shared_ff = shared_gate.shape[1]
    groups = len(ORDER)
    far = groups - NEAR
    hbm = pl.BlockSpec(memory_space=pl.ANY)
    vmem = pl.BlockSpec(memory_space=pltpu.VMEM)
    dma = pltpu.SemaphoreType.DMA

    def buf(*shape):
        return pltpu.VMEM(shape, BF16)

    def wide(*shape):
        return pltpu.VMEM(shape, F32)

    scratch = [
        buf(tokens, quarter),
        buf(tokens, quarter),
        buf(quarter, width),
        buf(tokens, width),
        buf(width, ff),
        buf(width, ff),
        buf(width, shared_ff),
        buf(width, shared_ff),
        buf(shared_ff, quarter),
        buf(tokens, width),
        buf(NEAR, BODY, width),
        buf(NEAR, 8, 8, 512),
        buf(far, BODY, quarter),
        buf(far, 8, 8, 128),
        buf(groups * ROWS, width),
        buf(NEAR, 8, 8, 512),
        buf(far, 8, 8, 128),
        buf(groups * ROWS, full_ff),
        buf(full_ff, quarter),
        buf(2, ff // 2, quarter),
        buf(groups, BODY, quarter),
        buf(groups, 8, 8, 128),
        buf(groups * ROWS, quarter),
        buf(groups, 8, 8, 128),
        wide(tokens, quarter),
        wide(quarter // 128, tokens + 32, 128),
        wide(quarter // 128, 32, 128),
        wide(quarter // 128, tokens, 128),
        wide(tokens, 128),
        wide(tokens, 128),
        buf(32, quarter),
        buf(32, quarter),
        wide(8, tokens),
        wide(4, 8, tokens),
        buf(tokens, quarter),
        buf(tokens, quarter),
        buf(tokens, quarter),
        buf(tokens, quarter),
        wide(tokens, quarter),
        buf(tokens // 2, quarter),
        buf(tokens // 2, quarter),
        buf(tokens, quarter),
        buf(tokens, quarter),
        dma((10,)),
        dma((groups,)),
        dma((groups,)),
        dma((groups,)),
        dma((groups,)),
        dma((groups,)),
        dma((groups,)),
        dma((groups,)),
        dma((groups,)),
        dma((2 * len(BATCHES), 4)),
        dma((2 * len(BATCHES), 4)),
        dma((6,)),
        dma((6,)),
        dma,
        dma,
        dma((3,)),
        dma((3,)),
        dma((6,)),
        dma((6,)),
    ]
    result = jax.ShapeDtypeStruct((tokens, quarter), BF16)
    return pl.pallas_call(
        kernel,
        out_shape=(result, result),
        in_specs=[hbm, hbm, vmem, vmem, hbm, hbm, vmem, vmem, vmem, hbm, hbm, hbm, hbm, hbm, hbm],
        out_specs=(vmem, vmem),
        scratch_shapes=scratch,
        compiler_params=pltpu.CompilerParams(collective_id=0, has_side_effects=True),
    )(
        conv_value,
        conv_gate,
        conv_taps,
        conv_gain.reshape(1, -1),
        conv_proj,
        moe_tokens,
        moe_gain.reshape(1, -1),
        routes.T,
        route_weights.T,
        expert_gate,
        expert_up,
        expert_down,
        shared_gate,
        shared_up,
        shared_down,
    )


def solution(mesh):
    placed = (
        P("ep", "tp"),
        P("ep", "tp"),
        P(None, "tp"),
        P("tp"),
        P("tp", None),
        P("ep", None),
        P(),
        P("ep", None),
        P("ep", None),
        P("ep", None, "tp"),
        P("ep", None, "tp"),
        P("ep", "tp", None),
        P(),
        P(),
        P(None, "tp"),
    )
    return jax.shard_map(
        local, mesh=mesh, in_specs=placed, out_specs=(P("ep", "tp"), P("ep", "tp")), check_vma=False
    )
```

time: 313 us -> 118 us (0.38)
  waiting for transfers between devices: 125 us -> 0 us
  Pallas kernels: 0 us -> 114 us
  blocking collectives: 70.7 us -> 0 us
  local copies, waits for them, and re-layouts: 45.9 us -> 3.53 us
  matrix products: 24.2 us -> 0 us
  other arithmetic: 16.4 us -> 0 us
  starting transfers between devices: 15.2 us -> 0 us
  between operations: 14 us -> 0.64 us
    pallas_call x0 -> x1, Pallas kernels: none -> 114 us  [local(): pl.pallas_call(kernel, out_shape=(result, result), in_specs=[hbm, hbm, vm...]
    all_gather x1 -> x0, waiting for transfers between devices: 64.9 us -> none  [local(): arrived = lax.all_gather(arrived, 'tp', axis=2, tiled=True)]
    all_to_all x1 -> x0, blocking collectives: 52.1 us -> none  [local(): lax.all_to_all(column_block, 'ep', split_axis=0, concat_axis=0, tiled=True)]
    all_to_all x1 -> x0, waiting for transfers between devices: 35.8 us -> none  [local(): lax.all_to_all(expert_rows, 'ep', split_axis=0, concat_axis=0, tiled=True)]
    dot_general x5 -> x0, matrix products: 24.2 us -> none  [the longest x1 10.3 us: local(): jnp.dot(hidden, expert_down[0], preferred_element_type=jnp.float32)]
    reduce_scatter x2 -> x0, waiting for transfers between devices: 23.5 us -> none  [the longest x1 23.5 us: local(): lax.psum_scatter(expert_partial.astype(jnp.bfloat16), 'tp', scatter_dimen...]
    gather x3 -> x0, local copies, waits for them, and re-layouts: 23.2 us -> none  [the longest x2 19.9 us: local(): normalized[token_index]]
    all_gather x2 -> x0, blocking collectives: 18.6 us -> none  [total_of_pieces(): parts = lax.all_gather(value, axis)]
  transfers between devices with their start and end apart: 5 -> 0, of which waited for: 4 -> 0; matrix products, arithmetic and copies ran while one was open for 9% -> 0% of each run, Pallas kernels for 0% -> 0%
where the time goes in v1:
time: 118 us
  Pallas kernels  114 us (97%)
  local copies, waits for them, and re-layouts  3.53 us (3%)
    pallas_call x1, Pallas kernels, local(): pl.pallas_call(kernel, out_shape=(result, result), in_specs=[hbm, hbm, vm...  114 us
    unnamed x2, local copies, waits for them, and re-layouts  3.53 us

profile of v1, /device:TPU:1, one launch (start us, length us, event | category | flops | bytes accessed | tf_op | source)
XLA Modules:
  0.0 118.2 jit_solution(7662718593169898226)
XLA Ops:
  0.6 114.0 %shard_map.158 = (bf16[384,512]{1,0:T(8,128)(2,1)}, bf16[384,512]{1,0:T(8,128)(2,1)}) custom-call(bf16[384,512]{1,0:T(8,128)(2,1)} %cv_hbm.1, bf16[384,512]{1,0:T(8,128)(2,1)} %cg_hbm.1, bf16[31,512]{1,0:T(8,128)(2,1)} %taps_ref.1, f32[1,512]{1,0:T(1,128)} %bitcast.7, bf16[512,2048]{1,0:T(8,128)(2,1)} %cproj_hbm.1, bf16[384,2048]{1,0:T(8,128)(2,1)} %tok_hbm.1, ...), custom_call_target="tpu_custom_call" | custom-call | tf_op jit(solution)/shard_map/pallas_call | solution.py:672
  114.7 1.8 %copy.19 = bf16[384,512]{1,0:T(8,128)(2,1)} copy(bf16[384,512]{1,0:T(8,128)(2,1)} %get-tuple-element.4) | data formatting | bytes 786432
  116.4 1.8 %copy.20 = bf16[384,512]{1,0:T(8,128)(2,1)} copy(bf16[384,512]{1,0:T(8,128)(2,1)} %get-tuple-element.5) | data formatting | bytes 786432

commit v2 on v1

--- a/solution.py
+++ b/solution.py
@@ -19,7 +19,7 @@
 ROWS = PLANE * (MAIN + REST)
 BODY = PLANE * MAIN
 NEAR = 3
-BATCHES = ((0, 3), (7, 1), (5, 2), (3, 2))
+SENT = (6, 7, 4, 5, 3, 2, 0, 1)
 
 
 def silu(v):
@@ -37,13 +37,13 @@
 def kernel(
     cv_hbm,
     cg_hbm,
-    taps_ref,
-    cgain_ref,
+    taps_hbm,
+    cgain_hbm,
     cproj_hbm,
     tok_hbm,
-    mgain_ref,
-    routes_ref,
-    weights_ref,
+    mgain_hbm,
+    routes_hbm,
+    weights_hbm,
     eg_hbm,
     eu_hbm,
     ed_hbm,
@@ -54,6 +54,11 @@
     moe_out,
     cv,
     cg,
+    taps_ref,
+    cgain_ref,
+    mgain_ref,
+    routes_ref,
+    weights_ref,
     cproj,
     tok,
     wg,
@@ -71,7 +76,6 @@
     in_far_rest,
     hid,
     down,
-    down_pass,
     back_send,
     back_send_rest,
     back,
@@ -161,8 +165,13 @@
     for number, (name, src, dst) in enumerate(
         (
             ("tok", tok_hbm, tok),
+            ("mgain", mgain_hbm, mgain_ref),
+            ("routes", routes_hbm, routes_ref),
             ("cv", cv_hbm, cv),
             ("cg", cg_hbm, cg),
+            ("taps", taps_hbm, taps_ref),
+            ("cgain", cgain_hbm, cgain_ref),
+            ("weights", weights_hbm, weights_ref),
             ("sg", sg_hbm, sg),
             ("su", su_hbm, su),
             ("sd", sd_hbm, sd),
@@ -175,18 +184,8 @@
         loads[name] = pltpu.make_async_copy(src, dst, load_sem.at[number])
         loads[name].start()
 
-    loads["cv"].wait()
-    loads["cg"].wait()
-    blocks = quarter // 128
-    extra = halo.shape[0]
-    for b in range(blocks):
-        lanes = slice(b * 128, (b + 1) * 128)
-        gated = (cv[:, lanes].astype(F32) * jax.nn.sigmoid(cg[:, lanes].astype(F32))).astype(BF16)
-        padded[b, extra:, :] = gated.astype(F32)
-        tail[:, lanes] = gated[tokens - extra :]
-        taps[b, 0:31] = taps_ref[:, lanes].astype(F32)
-
     loads["tok"].wait()
+    loads["mgain"].wait()
     for r in range(0, tokens, 64):
         rows = tok[r : r + 64, :].astype(F32)
         mean = jnp.sum(rows, axis=1, keepdims=True) * (1.0 / width)
@@ -194,22 +193,7 @@
         var = jnp.sum(centered * centered, axis=1, keepdims=True) * (1.0 / width)
         norm[r : r + 64, :] = (centered * lax.rsqrt(var + epsilon) * mgain_ref[...]).astype(BF16)
 
-    pl.semaphore_wait(barrier, n_ep - 1 + n_tp - 1)
-
-    next_ep = lax.rem(ep + 1, n_ep)
-    remote(tail, halo, halo_send, halo_recv, next_ep, tp).start()
-
-    half = ff // 2
-
-    def down_rows(owner, first, count):
-        return down.at[pl.ds(pl.multiple_of(owner * ff + first, half), count)]
-
-    ed = ed_hbm.at[0]
-    remote(ed.at[:, at_quarter(right)], down_rows(tp, 0, ff), down_send.at[0], down_recv.at[0], ep, right).start()
-    remote(ed.at[:, at_quarter(left)], down_rows(tp, 0, ff), down_send.at[1], down_recv.at[1], ep, left).start()
-    remote(ed.at[0:half, at_quarter(across)], down_pass.at[0], down_send.at[2], down_recv.at[2], ep, right).start()
-    remote(ed.at[half:ff, at_quarter(across)], down_pass.at[1], down_send.at[3], down_recv.at[3], ep, left).start()
-
+    loads["routes"].wait()
     routes = routes_ref[...]
     first, second = routes[0:1, :], routes[1:2, :]
     names = iota((n_ep, tokens), 0)
@@ -286,7 +270,31 @@
     def far_lanes():
         return at_quarter(tp)
 
-    for group in (0, 1, 2, 7, 5, 6, 3, 4):
+    loads["cv"].wait()
+    loads["cg"].wait()
+    loads["taps"].wait()
+    blocks = quarter // 128
+    extra = halo.shape[0]
+    for b in range(blocks):
+        lanes = slice(b * 128, (b + 1) * 128)
+        gated = (cv[:, lanes].astype(F32) * jax.nn.sigmoid(cg[:, lanes].astype(F32))).astype(BF16)
+        padded[b, extra:, :] = gated.astype(F32)
+        tail[:, lanes] = gated[tokens - extra :]
+        taps[b, 0:31] = taps_ref[:, lanes].astype(F32)
+
+    pl.semaphore_wait(barrier, n_ep - 1 + n_tp - 1)
+
+    next_ep = lax.rem(ep + 1, n_ep)
+    remote(tail, halo, halo_send, halo_recv, next_ep, tp).start()
+
+    def down_rows(owner):
+        return down.at[at_ff(owner)]
+
+    ed = ed_hbm.at[0]
+    remote(ed.at[:, at_quarter(right)], down_rows(tp), down_send.at[0], down_recv.at[0], ep, right).start()
+    remote(ed.at[:, at_quarter(left)], down_rows(tp), down_send.at[1], down_recv.at[1], ep, left).start()
+
+    for group in SENT:
         row = iota((ROWS, tokens), 0) + group * ROWS
         pick = ((row == slot_first) | (row == slot_second)).astype(F32).astype(BF16)
         if group < NEAR:
@@ -307,6 +315,106 @@
             xin[row_of(0, mine), :] = send_near[0, place_rows(mine), :]
             in_near_rest[0, mine] = send_near_rest[0, mine]
 
+    def parts_of(count):
+        cut = (count // 2 + 15) // 16 * 16
+        return (0, cut), (cut, count - cut)
+
+    def region(ref, lanes, first, rows, q):
+        return ref.at[first : first + rows, lanes(q)]
+
+    def gather_start(i, ref, lanes, first, count):
+        own = region(ref, lanes, first, count, tp)
+        remote(own, own, ag_send.at[i, 0], ag_recv.at[i, 0], ep, right).start()
+        remote(own, own, ag_send.at[i, 1], ag_recv.at[i, 1], ep, left).start()
+
+    def gather_pass(i, ref, lanes, first, count):
+        (a, na), (b, nb) = parts_of(count)
+        arrived(region(ref, lanes, first, count, left), ag_recv.at[i, 0])
+        half = region(ref, lanes, first + a, na, left)
+        remote(half, half, ag_send.at[i, 2], ag_recv.at[i, 2], ep, right).start()
+        arrived(region(ref, lanes, first, count, right), ag_recv.at[i, 1])
+        half = region(ref, lanes, first + b, nb, right)
+        remote(half, half, ag_send.at[i, 3], ag_recv.at[i, 3], ep, left).start()
+
+    def gather_end(i, ref, lanes, first, count):
+        (a, na), (b, nb) = parts_of(count)
+        arrived(region(ref, lanes, first + a, na, across), ag_recv.at[i, 2])
+        arrived(region(ref, lanes, first + b, nb, across), ag_recv.at[i, 3])
+
+    def gather_sent(i, ref, lanes, first, count):
+        (a, na), (b, nb) = parts_of(count)
+        left_here(region(ref, lanes, first, count, tp), ag_send.at[i, 0])
+        left_here(region(ref, lanes, first, count, tp), ag_send.at[i, 1])
+        left_here(region(ref, lanes, first + a, na, left), ag_send.at[i, 2])
+        left_here(region(ref, lanes, first + b, nb, right), ag_send.at[i, 3])
+
+    def rows_gather(step, group):
+        step(group, xin, at_quarter, group * ROWS, ROWS)
+
+    def hidden_gather(step, group):
+        step(len(ORDER) + group, hid, at_ff, group * ROWS, ROWS)
+
+    def come(group):
+        start = group * ROWS
+        if group < NEAR:
+            main, rest = xin.at[start : start + BODY], in_near_rest.at[group]
+        else:
+            main, rest = xin.at[start : start + BODY, far_lanes()], in_far_rest.at[group - NEAR]
+        sent_or_come(group, arrived, main, rest, go_recv, go_rest_recv)
+        if group < NEAR:
+            xin[start + BODY : start + ROWS, :] = unpack_rest(rest[...])
+        else:
+            xin[start + BODY : start + ROWS, far_lanes()] = unpack_rest(rest[...])
+
+    def hidden(group):
+        start = group * ROWS
+        rows = xin[start : start + ROWS, :]
+        value = silu(dot(rows, wg[...])) * dot(rows, wu[...])
+        hid[start : start + ROWS, at_ff(tp)] = value.astype(BF16)
+
+    def send_back(group):
+        start = group * ROWS
+        own = dot(hid[start : start + ROWS, :], down[...])
+        back_send[group] = own[0:BODY].astype(BF16)
+        back_send_rest[group] = pack_rest(own[BODY:]).astype(BF16)
+        exchange(
+            group,
+            -1,
+            back_send.at[group],
+            back.at[row_of(group, mine)],
+            back_send_rest.at[group],
+            back_rest.at[group, mine],
+            back_ssem,
+            back_rsem,
+            back_rest_ssem,
+            back_rest_rsem,
+        )
+        if group == 0:
+            back[row_of(0, mine), :] = back_send[0, place_rows(mine), :]
+            back_rest[0, mine] = back_send_rest[0, mine]
+
+    tall = iota((128, tokens), 0)
+    wide = jnp.where(tall == 0, slot_first.astype(F32), jnp.where(tall == 1, slot_second.astype(F32), 0.0))
+    loads["weights"].wait()
+    given = weights_ref[...]
+    wide = jnp.where(tall == 2, given[0:1, :], jnp.where(tall == 3, given[1:2, :], wide))
+    turned = wide.T
+    slot_one, slot_two = turned[:, 0:1].astype(jnp.int32), turned[:, 1:2].astype(jnp.int32)
+    weight_one, weight_two = turned[:, 2:3], turned[:, 3:4]
+
+    def combine(group):
+        start = group * ROWS
+        sent_or_come(
+            group, arrived, back.at[start : start + BODY], back_rest.at[group], back_rsem, back_rest_rsem
+        )
+        back[start + BODY : start + ROWS, :] = unpack_rest(back_rest[group])
+        lane = iota((tokens, ROWS), 1) + start
+        mix = jnp.where(lane == slot_one, weight_one, 0.0) + jnp.where(lane == slot_two, weight_two, 0.0)
+        high = mix.astype(BF16)
+        low = (mix - high.astype(F32)).astype(BF16)
+        rows = back[start : start + ROWS, :]
+        total[...] += dot(high, rows) + dot(low, rows)
+
     arrived(halo, halo_recv)
     for b in range(blocks):
         before_rows = halo[:, b * 128 : (b + 1) * 128].astype(F32)
@@ -334,21 +442,25 @@
     for i, peer in enumerate((right, left, across)):
         remote(stat_send, stat.at[tp], stat_ssem.at[i], stat_rsem.at[i], ep, peer).start()
 
+    remote(ed.at[:, at_quarter(across)], down_rows(tp), down_send.at[2], down_recv.at[2], ep, across).start()
+
     loads["sg"].wait()
     loads["su"].wait()
     loads["sd"].wait()
     shared = (silu(dot(norm[...], sg[...])) * dot(norm[...], su[...])).astype(BF16)
     total[...] = dot(shared, sd[...])
 
+    come(6)
+    rows_gather(gather_start, 6)
     for i, peer in enumerate((left, right, across)):
         arrived(stat.at[peer], stat_rsem.at[i])
     sums = stat[0] + stat[1] + stat[2] + stat[3]
     average = sums[0:1] * (1.0 / width)
     variance = sums[1:2] * (1.0 / width) - average * average
     scale = lax.rsqrt(variance + epsilon)
-    tall = iota((128, tokens), 0)
     turned = jnp.where(tall == 0, average, jnp.where(tall == 1, scale, 0.0)).T
     average, scale = turned[:, 0:1], turned[:, 1:2]
+    loads["cgain"].wait()
     for b in range(blocks):
         lanes = slice(b * 128, (b + 1) * 128)
         act[:, lanes] = silu((conv[b] - average) * scale * cgain_ref[:, lanes]).astype(BF16)
@@ -361,19 +473,68 @@
         return dot(act[...], cproj[:, at_quarter(q)])
 
     cfar[...] = product(across).astype(BF16)
+    cright[...] = product(right).astype(BF16)
+    cleft[...] = product(left).astype(BF16)
+    cown[...] = product(tp)
+
     remote(cfar.at[top], half_a, rs_send.at[0], rs_recv.at[0], ep, right).start()
     remote(cfar.at[bottom], half_b, rs_send.at[1], rs_recv.at[1], ep, left).start()
-    cright[...] = product(right).astype(BF16)
     remote(cright.at[bottom], from_left.at[bottom], rs_send.at[2], rs_recv.at[2], ep, right).start()
-    cleft[...] = product(left).astype(BF16)
     remote(cleft.at[top], from_right.at[top], rs_send.at[3], rs_recv.at[3], ep, left).start()
-    cown[...] = product(tp)
-
-    arrived(down_pass.at[0], down_recv.at[2])
-    remote(down_pass.at[0], down_rows(left, 0, half), down_send.at[4], down_recv.at[4], ep, right).start()
-    arrived(down_pass.at[1], down_recv.at[3])
-    remote(down_pass.at[1], down_rows(right, half, half), down_send.at[5], down_recv.at[5], ep, left).start()
-
+
+    come(7)
+    rows_gather(gather_start, 7)
+    rows_gather(gather_pass, 6)
+    come(4)
+    rows_gather(gather_start, 4)
+    rows_gather(gather_pass, 7)
+    rows_gather(gather_end, 6)
+    loads["wg"].wait()
+    loads["wu"].wait()
+    hidden(6)
+    hidden_gather(gather_start, 6)
+    rows_gather(gather_pass, 4)
+    come(5)
+    rows_gather(gather_start, 5)
+    rows_gather(gather_end, 7)
+    hidden(7)
+    hidden_gather(gather_start, 7)
+    hidden_gather(gather_pass, 6)
+    rows_gather(gather_pass, 5)
+    come(3)
+    rows_gather(gather_start, 3)
+    rows_gather(gather_end, 4)
+    hidden(4)
+    hidden_gather(gather_start, 4)
+    hidden_gather(gather_pass, 7)
+    loads["down"].wait()
+    arrived(down_rows(left), down_recv.at[0])
+    arrived(down_rows(right), down_recv.at[1])
+    arrived(down_rows(across), down_recv.at[2])
+    hidden_gather(gather_end, 6)
+    send_back(6)
+    rows_gather(gather_pass, 3)
+    hidden_gather(gather_pass, 4)
+    rows_gather(gather_end, 5)
+    hidden(5)
+    hidden_gather(gather_start, 5)
+    hidden_gather(gather_end, 7)
+    send_back(7)
+    rows_gather(gather_end, 3)
+    hidden(3)
+    hidden_gather(gather_start, 3)
+    hidden_gather(gather_end, 4)
+    send_back(4)
+    hidden_gather(gather_pass, 5)
+    come(0)
+    hidden(0)
+    hidden_gather(gather_start, 0)
+    come(2)
+    hidden(2)
+    hidden_gather(gather_start, 2)
+    hidden_gather(gather_pass, 3)
+    hidden_gather(gather_end, 5)
+    send_back(5)
     arrived(half_a, rs_recv.at[0])
     cright[top] = (cright[top].astype(F32) + half_a[...].astype(F32)).astype(BF16)
     remote(cright.at[top], from_left.at[top], rs_send.at[4], rs_recv.at[4], ep, right).start()
@@ -381,157 +542,25 @@
     cleft[bottom] = (cleft[bottom].astype(F32) + half_b[...].astype(F32)).astype(BF16)
     remote(cleft.at[bottom], from_right.at[bottom], rs_send.at[5], rs_recv.at[5], ep, left).start()
 
-    def parts_of(count):
-        cut = (count // 2 + 15) // 16 * 16
-        return (0, cut), (cut, count - cut)
-
-    def region(ref, lanes, first, rows, q):
-        return ref.at[first : first + rows, lanes(q)]
-
-    def gather_start(i, ref, lanes, first, count):
-        own = region(ref, lanes, first, count, tp)
-        remote(own, own, ag_send.at[i, 0], ag_recv.at[i, 0], ep, right).start()
-        remote(own, own, ag_send.at[i, 1], ag_recv.at[i, 1], ep, left).start()
-
-    def gather_pass(i, ref, lanes, first, count):
-        (a, na), (b, nb) = parts_of(count)
-        arrived(region(ref, lanes, first, count, left), ag_recv.at[i, 0])
-        half = region(ref, lanes, first + a, na, left)
-        remote(half, half, ag_send.at[i, 2], ag_recv.at[i, 2], ep, right).start()
-        arrived(region(ref, lanes, first, count, right), ag_recv.at[i, 1])
-        half = region(ref, lanes, first + b, nb, right)
-        remote(half, half, ag_send.at[i, 3], ag_recv.at[i, 3], ep, left).start()
-
-    def gather_end(i, ref, lanes, first, count):
-        (a, na), (b, nb) = parts_of(count)
-        arrived(region(ref, lanes, first + a, na, across), ag_recv.at[i, 2])
-        arrived(region(ref, lanes, first + b, nb, across), ag_recv.at[i, 3])
-
-    def gather_sent(i, ref, lanes, first, count):
-        (a, na), (b, nb) = parts_of(count)
-        left_here(region(ref, lanes, first, count, tp), ag_send.at[i, 0])
-        left_here(region(ref, lanes, first, count, tp), ag_send.at[i, 1])
-        left_here(region(ref, lanes, first + a, na, left), ag_send.at[i, 2])
-        left_here(region(ref, lanes, first + b, nb, right), ag_send.at[i, 3])
-
-    def of_batch(batch):
-        first, count = BATCHES[batch]
-        return first * ROWS, count * ROWS
-
-    def rows_gather(step, batch):
-        step(batch, xin, at_quarter, *of_batch(batch))
-
-    def hidden_gather(step, batch):
-        step(len(BATCHES) + batch, hid, at_ff, *of_batch(batch))
-
-    def come(batch):
-        first, count = BATCHES[batch]
-        for group in range(first, first + count):
-            start = group * ROWS
-            if group < NEAR:
-                main, rest = xin.at[start : start + BODY], in_near_rest.at[group]
-            else:
-                main, rest = xin.at[start : start + BODY, far_lanes()], in_far_rest.at[group - NEAR]
-            sent_or_come(group, arrived, main, rest, go_recv, go_rest_recv)
-            if group < NEAR:
-                xin[start + BODY : start + ROWS, :] = unpack_rest(rest[...])
-            else:
-                xin[start + BODY : start + ROWS, far_lanes()] = unpack_rest(rest[...])
-
-    def hidden(batch):
-        first, count = of_batch(batch)
-        rows = xin[first : first + count, :]
-        value = silu(dot(rows, wg[...])) * dot(rows, wu[...])
-        hid[first : first + count, at_ff(tp)] = value.astype(BF16)
-
-    def send_back(batch):
-        first, count = BATCHES[batch]
-        start = first * ROWS
-        rows = dot(hid[start : start + count * ROWS, :], down[...])
-        for group in range(first, first + count):
-            own = rows[(group - first) * ROWS : (group - first + 1) * ROWS]
-            back_send[group] = own[0:BODY].astype(BF16)
-            back_send_rest[group] = pack_rest(own[BODY:]).astype(BF16)
-            exchange(
-                group,
-                -1,
-                back_send.at[group],
-                back.at[row_of(group, mine)],
-                back_send_rest.at[group],
-                back_rest.at[group, mine],
-                back_ssem,
-                back_rsem,
-                back_rest_ssem,
-                back_rest_rsem,
-            )
-            if group == 0:
-                back[row_of(0, mine), :] = back_send[0, place_rows(mine), :]
-                back_rest[0, mine] = back_send_rest[0, mine]
-
-    wide = jnp.where(tall == 0, slot_first.astype(F32), jnp.where(tall == 1, slot_second.astype(F32), 0.0))
-    given = weights_ref[...]
-    wide = jnp.where(tall == 2, given[0:1, :], jnp.where(tall == 3, given[1:2, :], wide))
-    turned = wide.T
-    slot_one, slot_two = turned[:, 0:1].astype(jnp.int32), turned[:, 1:2].astype(jnp.int32)
-    weight_one, weight_two = turned[:, 2:3], turned[:, 3:4]
-
-    def combine(batch):
-        first, count = BATCHES[batch]
-        for group in range(first, first + count):
-            start = group * ROWS
-            sent_or_come(
-                group, arrived, back.at[start : start + BODY], back_rest.at[group], back_rsem, back_rest_rsem
-            )
-            back[start + BODY : start + ROWS, :] = unpack_rest(back_rest[group])
-        start = first * ROWS
-        lane = iota((tokens, count * ROWS), 1) + start
-        mix = jnp.where(lane == slot_one, weight_one, 0.0) + jnp.where(lane == slot_two, weight_two, 0.0)
-        high = mix.astype(BF16)
-        low = (mix - high.astype(F32)).astype(BF16)
-        rows = back[start : start + count * ROWS, :]
-        total[...] += dot(high, rows) + dot(low, rows)
-
-    come(0)
-    loads["wg"].wait()
-    loads["wu"].wait()
-    hidden(0)
-    hidden_gather(gather_start, 0)
     come(1)
-    rows_gather(gather_start, 1)
+    hidden(1)
+    hidden_gather(gather_start, 1)
+    hidden_gather(gather_end, 3)
+    send_back(3)
     hidden_gather(gather_pass, 0)
-    come(2)
-    rows_gather(gather_start, 2)
-    rows_gather(gather_pass, 1)
-    come(3)
-    rows_gather(gather_start, 3)
-
-    loads["down"].wait()
-    arrived(down_rows(left, 0, ff), down_recv.at[0])
-    arrived(down_rows(right, 0, ff), down_recv.at[1])
-    arrived(down_rows(across, 0, half), down_recv.at[4])
-    arrived(down_rows(across, half, half), down_recv.at[5])
+    hidden_gather(gather_pass, 2)
     hidden_gather(gather_end, 0)
     send_back(0)
-
-    rows_gather(gather_end, 1)
-    hidden(1)
-    hidden_gather(gather_start, 1)
-    rows_gather(gather_pass, 2)
-    rows_gather(gather_pass, 3)
-    rows_gather(gather_end, 2)
-    hidden(2)
-    hidden_gather(gather_start, 2)
+    hidden_gather(gather_end, 2)
+    send_back(2)
     hidden_gather(gather_pass, 1)
+    combine(6)
+    combine(7)
     hidden_gather(gather_end, 1)
     send_back(1)
-    rows_gather(gather_end, 3)
-    hidden(3)
-    hidden_gather(gather_start, 3)
-    hidden_gather(gather_pass, 2)
-    hidden_gather(gather_end, 2)
-    send_back(2)
-    hidden_gather(gather_pass, 3)
-
+    combine(4)
+    combine(5)
+    combine(3)
     arrived(from_left.at[bottom], rs_recv.at[2])
     arrived(from_right.at[top], rs_recv.at[3])
     arrived(from_left.at[top], rs_recv.at[4])
@@ -539,20 +568,13 @@
     conv_out[...] = (cown[...] + from_left[...].astype(F32) + from_right[...].astype(F32)).astype(BF16)
 
     combine(0)
-    hidden_gather(gather_end, 3)
-    send_back(3)
+    combine(2)
     combine(1)
-    combine(2)
-    combine(3)
     moe_out[...] = total[...].astype(BF16)
-
     left_here(tail, halo_send)
     left_here(ed.at[:, at_quarter(right)], down_send.at[0])
     left_here(ed.at[:, at_quarter(left)], down_send.at[1])
-    left_here(ed.at[0:half, at_quarter(across)], down_send.at[2])
-    left_here(ed.at[half:ff, at_quarter(across)], down_send.at[3])
-    left_here(down_pass.at[0], down_send.at[4])
-    left_here(down_pass.at[1], down_send.at[5])
+    left_here(ed.at[:, at_quarter(across)], down_send.at[2])
     for i in range(3):
         left_here(stat_send, stat_ssem.at[i])
     for i, part in enumerate((cfar.at[top], cfar.at[bottom], cright.at[bottom], cleft.at[top], cright.at[top], cleft.at[bottom])):
@@ -564,10 +586,14 @@
             main, rest = send_far.at[group - NEAR], send_far_rest.at[group - NEAR]
         sent_or_come(group, left_here, main, rest, go_send, go_rest_send)
         sent_or_come(group, left_here, back_send.at[group], back_send_rest.at[group], back_ssem, back_rest_ssem)
-    for batch in range(len(BATCHES)):
-        if batch > 0:
-            rows_gather(gather_sent, batch)
-        hidden_gather(gather_sent, batch)
+        if group >= NEAR:
+            rows_gather(gather_sent, group)
+        hidden_gather(gather_sent, group)
+
+
+def handed_on(a_ref, b_ref, a_out, b_out):
+    a_out[...] = a_ref[...]
+    b_out[...] = b_ref[...]
 
 
 def local(
@@ -607,6 +633,11 @@
     scratch = [
         buf(tokens, quarter),
         buf(tokens, quarter),
+        buf(31, quarter),
+        wide(1, quarter),
+        wide(1, width),
+        pltpu.VMEM((2, tokens), jnp.int32),
+        wide(2, tokens),
         buf(quarter, width),
         buf(tokens, width),
         buf(width, ff),
@@ -624,7 +655,6 @@
         buf(far, 8, 8, 128),
         buf(groups * ROWS, full_ff),
         buf(full_ff, quarter),
-        buf(2, ff // 2, quarter),
         buf(groups, BODY, quarter),
         buf(groups, 8, 8, 128),
         buf(groups * ROWS, quarter),
@@ -648,7 +678,7 @@
         buf(tokens // 2, quarter),
         buf(tokens, quarter),
         buf(tokens, quarter),
-        dma((10,)),
+        dma((15,)),
         dma((groups,)),
         dma((groups,)),
         dma((groups,)),
@@ -657,10 +687,10 @@
         dma((groups,)),
         dma((groups,)),
         dma((groups,)),
-        dma((2 * len(BATCHES), 4)),
-        dma((2 * len(BATCHES), 4)),
-        dma((6,)),
-        dma((6,)),
+        dma((2 * groups, 4)),
+        dma((2 * groups, 4)),
+        dma((3,)),
+        dma((3,)),
         dma,
         dma,
         dma((3,)),
@@ -669,10 +699,10 @@
         dma((6,)),
     ]
     result = jax.ShapeDtypeStruct((tokens, quarter), BF16)
-    return pl.pallas_call(
+    results = pl.pallas_call(
         kernel,
         out_shape=(result, result),
-        in_specs=[hbm, hbm, vmem, vmem, hbm, hbm, vmem, vmem, vmem, hbm, hbm, hbm, hbm, hbm, hbm],
+        in_specs=[hbm] * 15,
         out_specs=(vmem, vmem),
         scratch_shapes=scratch,
         compiler_params=pltpu.CompilerParams(collective_id=0, has_side_effects=True),
@@ -693,6 +723,9 @@
         shared_up,
         shared_down,
     )
+    return pl.pallas_call(
+        handed_on, out_shape=(result, result), in_specs=[vmem, vmem], out_specs=(vmem, vmem)
+    )(*results)
 
 
 def solution(mesh):

time: 118 us -> 102 us (0.86)
  Pallas kernels: 114 us -> 101 us
  local copies, waits for them, and re-layouts: 3.53 us -> 0 us
    pallas_call x1 -> x2, Pallas kernels: 114 us -> 101 us  [the longest x1 99.4 us: local(): pl.pallas_call(kernel, out_shape=(result, result), in_specs=[hbm] * 15, o...]
    unnamed x2 -> x0, local copies, waits for them, and re-layouts: 3.53 us -> none
where the time goes in v2:
time: 102 us
  Pallas kernels  101 us (99%)
    pallas_call x1, Pallas kernels, local(): pl.pallas_call(kernel, out_shape=(result, result), in_specs=[hbm] * 15, o...  99.4 us

profile of v2, /device:TPU:1, one launch (start us, length us, event | category | flops | bytes accessed | tf_op | source)
XLA Modules:
  0.0 102.1 jit_solution(16960277240774658973)
XLA Ops:
  0.6 99.4 %shard_map.158 = (bf16[384,512]{1,0:T(8,128)(2,1)}, bf16[384,512]{1,0:T(8,128)(2,1)}) custom-call(bf16[384,512]{1,0:T(8,128)(2,1)} %cv_hbm.1, bf16[384,512]{1,0:T(8,128)(2,1)} %cg_hbm.1, bf16[31,512]{1,0:T(8,128)(2,1)} %taps_hbm.1, f32[1,512]{1,0:T(1,128)} %bitcast.7, bf16[512,2048]{1,0:T(8,128)(2,1)} %cproj_hbm.1, bf16[384,2048]{1,0:T(8,128)(2,1)} %tok_hbm.1, ...), custom_call_target="tpu_custom_call" | custom-call | tf_op jit(solution)/shard_map/pallas_call | solution.py:702
  100.1 2.0 %shard_map.159 = (bf16[384,512]{1,0:T(8,128)(2,1)}, bf16[384,512]{1,0:T(8,128)(2,1)}) custom-call(bf16[384,512]{1,0:T(8,128)(2,1)} %get-tuple-element.4.a_ref, bf16[384,512]{1,0:T(8,128)(2,1)} %get-tuple-element.5.b_ref), custom_call_target="tpu_custom_call" | custom-call | tf_op jit(solution)/shard_map/pallas_call | solution.py:726

commit v3 on v2

--- a/solution.py
+++ b/solution.py
@@ -19,7 +19,7 @@
 ROWS = PLANE * (MAIN + REST)
 BODY = PLANE * MAIN
 NEAR = 3
-SENT = (6, 7, 4, 5, 3, 2, 0, 1)
+SENT = (7, 5, 6, 3, 4, 2, 1, 0)
 
 
 def silu(v):
@@ -450,8 +450,8 @@
     shared = (silu(dot(norm[...], sg[...])) * dot(norm[...], su[...])).astype(BF16)
     total[...] = dot(shared, sd[...])
 
-    come(6)
-    rows_gather(gather_start, 6)
+    come(7)
+    rows_gather(gather_start, 7)
     for i, peer in enumerate((left, right, across)):
         arrived(stat.at[peer], stat_rsem.at[i])
     sums = stat[0] + stat[1] + stat[2] + stat[3]
@@ -479,97 +479,94 @@
 
     remote(cfar.at[top], half_a, rs_send.at[0], rs_recv.at[0], ep, right).start()
     remote(cfar.at[bottom], half_b, rs_send.at[1], rs_recv.at[1], ep, left).start()
-    remote(cright.at[bottom], from_left.at[bottom], rs_send.at[2], rs_recv.at[2], ep, right).start()
-    remote(cleft.at[top], from_right.at[top], rs_send.at[3], rs_recv.at[3], ep, left).start()
-
-    come(7)
-    rows_gather(gather_start, 7)
-    rows_gather(gather_pass, 6)
-    come(4)
-    rows_gather(gather_start, 4)
+    come(5)
+    rows_gather(gather_start, 5)
     rows_gather(gather_pass, 7)
-    rows_gather(gather_end, 6)
+    come(6)
+    rows_gather(gather_start, 6)
+    rows_gather(gather_end, 7)
     loads["wg"].wait()
     loads["wu"].wait()
-    hidden(6)
-    hidden_gather(gather_start, 6)
-    rows_gather(gather_pass, 4)
-    come(5)
-    rows_gather(gather_start, 5)
-    rows_gather(gather_end, 7)
     hidden(7)
     hidden_gather(gather_start, 7)
-    hidden_gather(gather_pass, 6)
     rows_gather(gather_pass, 5)
     come(3)
     rows_gather(gather_start, 3)
-    rows_gather(gather_end, 4)
-    hidden(4)
-    hidden_gather(gather_start, 4)
+    rows_gather(gather_pass, 6)
+    rows_gather(gather_end, 5)
+    hidden(5)
+    hidden_gather(gather_start, 5)
     hidden_gather(gather_pass, 7)
+    come(4)
+    rows_gather(gather_start, 4)
+    rows_gather(gather_pass, 3)
+    rows_gather(gather_end, 6)
+    hidden(6)
+    hidden_gather(gather_start, 6)
+    hidden_gather(gather_pass, 5)
     loads["down"].wait()
     arrived(down_rows(left), down_recv.at[0])
     arrived(down_rows(right), down_recv.at[1])
     arrived(down_rows(across), down_recv.at[2])
-    hidden_gather(gather_end, 6)
-    send_back(6)
-    rows_gather(gather_pass, 3)
-    hidden_gather(gather_pass, 4)
-    rows_gather(gather_end, 5)
-    hidden(5)
-    hidden_gather(gather_start, 5)
     hidden_gather(gather_end, 7)
     send_back(7)
+    rows_gather(gather_pass, 4)
+    hidden_gather(gather_pass, 6)
     rows_gather(gather_end, 3)
     hidden(3)
     hidden_gather(gather_start, 3)
-    hidden_gather(gather_end, 4)
-    send_back(4)
-    hidden_gather(gather_pass, 5)
+    hidden_gather(gather_end, 5)
+    send_back(5)
+    rows_gather(gather_end, 4)
+    hidden(4)
+    hidden_gather(gather_start, 4)
+    hidden_gather(gather_end, 6)
+    send_back(6)
+    hidden_gather(gather_pass, 3)
+    come(2)
+    hidden(2)
+    hidden_gather(gather_start, 2)
+    come(1)
+    hidden(1)
+    hidden_gather(gather_start, 1)
+    hidden_gather(gather_pass, 4)
+    hidden_gather(gather_end, 3)
+    send_back(3)
     come(0)
     hidden(0)
     hidden_gather(gather_start, 0)
-    come(2)
-    hidden(2)
-    hidden_gather(gather_start, 2)
-    hidden_gather(gather_pass, 3)
-    hidden_gather(gather_end, 5)
-    send_back(5)
+    hidden_gather(gather_end, 4)
+    send_back(4)
+    hidden_gather(gather_pass, 2)
+    hidden_gather(gather_pass, 1)
+    remote(cright.at[bottom], from_left.at[bottom], rs_send.at[2], rs_recv.at[2], ep, right).start()
+    remote(cleft.at[top], from_right.at[top], rs_send.at[3], rs_recv.at[3], ep, left).start()
+    hidden_gather(gather_pass, 0)
     arrived(half_a, rs_recv.at[0])
     cright[top] = (cright[top].astype(F32) + half_a[...].astype(F32)).astype(BF16)
     remote(cright.at[top], from_left.at[top], rs_send.at[4], rs_recv.at[4], ep, right).start()
     arrived(half_b, rs_recv.at[1])
     cleft[bottom] = (cleft[bottom].astype(F32) + half_b[...].astype(F32)).astype(BF16)
     remote(cleft.at[bottom], from_right.at[bottom], rs_send.at[5], rs_recv.at[5], ep, left).start()
-
-    come(1)
-    hidden(1)
-    hidden_gather(gather_start, 1)
-    hidden_gather(gather_end, 3)
-    send_back(3)
-    hidden_gather(gather_pass, 0)
-    hidden_gather(gather_pass, 2)
+    hidden_gather(gather_end, 2)
+    send_back(2)
+    hidden_gather(gather_end, 1)
+    send_back(1)
     hidden_gather(gather_end, 0)
     send_back(0)
-    hidden_gather(gather_end, 2)
-    send_back(2)
-    hidden_gather(gather_pass, 1)
+    combine(7)
+    combine(5)
     combine(6)
-    combine(7)
-    hidden_gather(gather_end, 1)
-    send_back(1)
+    combine(3)
     combine(4)
-    combine(5)
-    combine(3)
+    combine(2)
+    combine(1)
+    combine(0)
     arrived(from_left.at[bottom], rs_recv.at[2])
     arrived(from_right.at[top], rs_recv.at[3])
     arrived(from_left.at[top], rs_recv.at[4])
     arrived(from_right.at[bottom], rs_recv.at[5])
     conv_out[...] = (cown[...] + from_left[...].astype(F32) + from_right[...].astype(F32)).astype(BF16)
-
-    combine(0)
-    combine(2)
-    combine(1)
     moe_out[...] = total[...].astype(BF16)
     left_here(tail, halo_send)
     left_here(ed.at[:, at_quarter(right)], down_send.at[0])

time: 102 us -> 94.6 us (0.927)
  Pallas kernels: 101 us -> 93.9 us
    pallas_call x1, Pallas kernels: 99.4 us -> 91.9 us  [local(): pl.pallas_call(kernel, out_shape=(result, result), in_specs=[hbm] * 15, o...]
where the time goes in v3:
time: 94.6 us; the launch traced here: 94.5 us
  Pallas kernels  93.9 us (99%)
    pallas_call x1, Pallas kernels, local(): pl.pallas_call(kernel, out_shape=(result, result), in_specs=[hbm] * 15, o...  91.9 us
    pallas_call x1, Pallas kernels, local(): pl.pallas_call(handed_on, out_shape=(result, result), in_specs=[vmem, vme...  2.02 us

profile of v3, /device:TPU:1, one launch (start us, length us, event | category | flops | bytes accessed | tf_op | source)
XLA Modules:
  0.0 94.5 jit_solution(4037624988576528843)
XLA Ops:
  0.6 91.9 %shard_map.158 = (bf16[384,512]{1,0:T(8,128)(2,1)}, bf16[384,512]{1,0:T(8,128)(2,1)}) custom-call(bf16[384,512]{1,0:T(8,128)(2,1)} %cv_hbm.1, bf16[384,512]{1,0:T(8,128)(2,1)} %cg_hbm.1, bf16[31,512]{1,0:T(8,128)(2,1)} %taps_hbm.1, f32[1,512]{1,0:T(1,128)} %bitcast.7, bf16[512,2048]{1,0:T(8,128)(2,1)} %cproj_hbm.1, bf16[384,2048]{1,0:T(8,128)(2,1)} %tok_hbm.1, ...), custom_call_target="tpu_custom_call" | custom-call | tf_op jit(solution)/shard_map/pallas_call | solution.py:699
  92.5 2.0 %shard_map.159 = (bf16[384,512]{1,0:T(8,128)(2,1)}, bf16[384,512]{1,0:T(8,128)(2,1)}) custom-call(bf16[384,512]{1,0:T(8,128)(2,1)} %get-tuple-element.4.a_ref, bf16[384,512]{1,0:T(8,128)(2,1)} %get-tuple-element.5.b_ref), custom_call_target="tpu_custom_call" | custom-call | tf_op jit(solution)/shard_map/pallas_call | solution.py:723

commit v4 on v3

--- a/solution.py
+++ b/solution.py
@@ -479,9 +479,9 @@
 
     remote(cfar.at[top], half_a, rs_send.at[0], rs_recv.at[0], ep, right).start()
     remote(cfar.at[bottom], half_b, rs_send.at[1], rs_recv.at[1], ep, left).start()
+    rows_gather(gather_pass, 7)
     come(5)
     rows_gather(gather_start, 5)
-    rows_gather(gather_pass, 7)
     come(6)
     rows_gather(gather_start, 6)
     rows_gather(gather_end, 7)
@@ -490,20 +490,18 @@
     hidden(7)
     hidden_gather(gather_start, 7)
     rows_gather(gather_pass, 5)
-    come(3)
-    rows_gather(gather_start, 3)
+    come(4)
+    rows_gather(gather_start, 4)
     rows_gather(gather_pass, 6)
     rows_gather(gather_end, 5)
     hidden(5)
     hidden_gather(gather_start, 5)
     hidden_gather(gather_pass, 7)
-    come(4)
-    rows_gather(gather_start, 4)
-    rows_gather(gather_pass, 3)
+    come(3)
+    rows_gather(gather_start, 3)
     rows_gather(gather_end, 6)
     hidden(6)
     hidden_gather(gather_start, 6)
-    hidden_gather(gather_pass, 5)
     loads["down"].wait()
     arrived(down_rows(left), down_recv.at[0])
     arrived(down_rows(right), down_recv.at[1])
@@ -511,62 +509,64 @@
     hidden_gather(gather_end, 7)
     send_back(7)
     rows_gather(gather_pass, 4)
+    hidden_gather(gather_pass, 5)
     hidden_gather(gather_pass, 6)
+    come(1)
+    hidden(1)
+    hidden_gather(gather_start, 1)
+    rows_gather(gather_pass, 3)
+    hidden_gather(gather_end, 5)
+    send_back(5)
+    hidden_gather(gather_end, 6)
+    send_back(6)
+    rows_gather(gather_end, 4)
+    hidden(4)
+    hidden_gather(gather_start, 4)
+    hidden_gather(gather_pass, 1)
+    come(2)
+    hidden(2)
+    hidden_gather(gather_start, 2)
     rows_gather(gather_end, 3)
     hidden(3)
     hidden_gather(gather_start, 3)
-    hidden_gather(gather_end, 5)
-    send_back(5)
-    rows_gather(gather_end, 4)
-    hidden(4)
-    hidden_gather(gather_start, 4)
-    hidden_gather(gather_end, 6)
-    send_back(6)
-    hidden_gather(gather_pass, 3)
-    come(2)
-    hidden(2)
-    hidden_gather(gather_start, 2)
-    come(1)
-    hidden(1)
-    hidden_gather(gather_start, 1)
     hidden_gather(gather_pass, 4)
-    hidden_gather(gather_end, 3)
-    send_back(3)
     come(0)
     hidden(0)
     hidden_gather(gather_start, 0)
+    hidden_gather(gather_pass, 3)
+    hidden_gather(gather_end, 1)
+    send_back(1)
     hidden_gather(gather_end, 4)
     send_back(4)
     hidden_gather(gather_pass, 2)
-    hidden_gather(gather_pass, 1)
+    combine(7)
+    hidden_gather(gather_pass, 0)
     remote(cright.at[bottom], from_left.at[bottom], rs_send.at[2], rs_recv.at[2], ep, right).start()
     remote(cleft.at[top], from_right.at[top], rs_send.at[3], rs_recv.at[3], ep, left).start()
-    hidden_gather(gather_pass, 0)
+    hidden_gather(gather_end, 3)
+    send_back(3)
+    hidden_gather(gather_end, 2)
+    send_back(2)
     arrived(half_a, rs_recv.at[0])
     cright[top] = (cright[top].astype(F32) + half_a[...].astype(F32)).astype(BF16)
     remote(cright.at[top], from_left.at[top], rs_send.at[4], rs_recv.at[4], ep, right).start()
     arrived(half_b, rs_recv.at[1])
     cleft[bottom] = (cleft[bottom].astype(F32) + half_b[...].astype(F32)).astype(BF16)
     remote(cleft.at[bottom], from_right.at[bottom], rs_send.at[5], rs_recv.at[5], ep, left).start()
-    hidden_gather(gather_end, 2)
-    send_back(2)
-    hidden_gather(gather_end, 1)
-    send_back(1)
     hidden_gather(gather_end, 0)
     send_back(0)
-    combine(7)
+    combine(4)
     combine(5)
     combine(6)
-    combine(3)
-    combine(4)
-    combine(2)
     combine(1)
     combine(0)
+    combine(3)
     arrived(from_left.at[bottom], rs_recv.at[2])
     arrived(from_right.at[top], rs_recv.at[3])
     arrived(from_left.at[top], rs_recv.at[4])
     arrived(from_right.at[bottom], rs_recv.at[5])
     conv_out[...] = (cown[...] + from_left[...].astype(F32) + from_right[...].astype(F32)).astype(BF16)
+    combine(2)
     moe_out[...] = total[...].astype(BF16)
     left_here(tail, halo_send)
     left_here(ed.at[:, at_quarter(right)], down_send.at[0])

time: 94.6 us -> 91.9 us (0.971)
  Pallas kernels: 93.9 us -> 91.2 us
    pallas_call x1, Pallas kernels: 91.9 us -> 89.1 us  [local(): pl.pallas_call(kernel, out_shape=(result, result), in_specs=[hbm] * 15, o...]
where the time goes in v4:
time: 91.9 us; the launch traced here: 91.8 us
  Pallas kernels  91.2 us (99%)
    pallas_call x1, Pallas kernels, local(): pl.pallas_call(kernel, out_shape=(result, result), in_specs=[hbm] * 15, o...  89.1 us
    pallas_call x1, Pallas kernels, local(): pl.pallas_call(handed_on, out_shape=(result, result), in_specs=[vmem, vme...  2.02 us

profile of v4, /device:TPU:1, one launch (start us, length us, event | category | flops | bytes accessed | tf_op | source)
XLA Modules:
  0.0 91.8 jit_solution(11610935866639386597)
XLA Ops:
  0.6 89.1 %shard_map.158 = (bf16[384,512]{1,0:T(8,128)(2,1)}, bf16[384,512]{1,0:T(8,128)(2,1)}) custom-call(bf16[384,512]{1,0:T(8,128)(2,1)} %cv_hbm.1, bf16[384,512]{1,0:T(8,128)(2,1)} %cg_hbm.1, bf16[31,512]{1,0:T(8,128)(2,1)} %taps_hbm.1, f32[1,512]{1,0:T(1,128)} %bitcast.7, bf16[512,2048]{1,0:T(8,128)(2,1)} %cproj_hbm.1, bf16[384,2048]{1,0:T(8,128)(2,1)} %tok_hbm.1, ...), custom_call_target="tpu_custom_call" | custom-call | tf_op jit(solution)/shard_map/pallas_call | solution.py:699
  89.8 2.0 %shard_map.159 = (bf16[384,512]{1,0:T(8,128)(2,1)}, bf16[384,512]{1,0:T(8,128)(2,1)}) custom-call(bf16[384,512]{1,0:T(8,128)(2,1)} %get-tuple-element.4.a_ref, bf16[384,512]{1,0:T(8,128)(2,1)} %get-tuple-element.5.b_ref), custom_call_target="tpu_custom_call" | custom-call | tf_op jit(solution)/shard_map/pallas_call | solution.py:723
